TPU v7x, 128 devices: a whole 4x4x4 slice. The times are simulated.
128 devices in a mesh: ep: 64 (over z, y, x), tp: 2 (over core).
Axes of the slice: x: 4, y: 4, z: 4, core: 2. Of those that a mesh axis runs over, the one named last changes fastest.
Arguments:
- tokens: bfloat16 [32768, 2048], P(('ep', 'tp')), may hold values from -6 to 6
- norm_gain: float32 [2048], replicated, may hold values from 0.1 to 1.9
- norm_bias: float32 [2048], replicated, may hold values from -3 to 3
- gate_weight: bfloat16 [64, 2048, 1024], P('ep', None, 'tp'), may hold values from -0.125 to 0.125
- up_weight: bfloat16 [64, 2048, 1024], P('ep', None, 'tp'), may hold values from -0.125 to 0.125
- down_weight: bfloat16 [64, 1024, 2048], P('ep', 'tp'), may hold values from -0.1875 to 0.1875
- expert_ids: int32 [32768, 2], P(('ep', 'tp')), may hold values from 0 to 63, all different within a row; in each aligned block of 256 rows (0 to 255, 256 to 511, ...) at most 16 rows name the same one
- route_weights: float32 [32768, 2], P(('ep', 'tp')), may hold values from 0.2 to 1
Outputs:
- mixed: bfloat16 [32768, 2048], P(('ep', 'tp'))
Inputs may be any that keep to these rules, and one draw needn't show every extreme that they name: `expert_ids`: a token's 2 experts differ; in the tokens of one device (aligned blocks of 256 rows) no expert is named by more than 16 entries, a bound that some block reaches.
All inputs are finite; a program needn't handle non-finite values.
Results may differ from a plain program's by a relative error of at most 0.0071.
Values may be sent and summed in bfloat16 or wider, within the bound.
No kernel may reach another device: no remote copies, remote signals or barrier semaphores. Data moves between devices by JAX's collectives and lax.ppermute only.
A program may use at most 128 MiB of HBM per device.

v0:
```python
import jax
import jax.numpy as jnp
from jax import lax
from jax.sharding import PartitionSpec as P


def body(
    tokens, norm_gain, norm_bias, gate_weight, up_weight, down_weight, expert_ids, route_weights
):
    tok_rows, width = tokens.shape
    topk = expert_ids.shape[1]
    experts = lax.axis_size("ep")
    capacity = max(4 * tok_rows // experts, 4)
    values = tokens.astype(jnp.float32)
    centre = values - jnp.mean(values, axis=-1, keepdims=True)
    spread = jnp.mean(centre * centre, axis=-1, keepdims=True)
    normed = (centre * lax.rsqrt(spread + 1e-05) * norm_gain + norm_bias).astype(jnp.bfloat16)
    flat_ids = expert_ids.reshape(-1)
    onehot = (flat_ids[:, None] == jnp.arange(experts, dtype=jnp.int32)[None, :]).astype(jnp.int32)
    slot = jnp.sum(jnp.cumsum(onehot, axis=0) * onehot, axis=1) - 1
    target = flat_ids * capacity + slot
    buffer = (
        jnp.zeros((experts * capacity, width), jnp.bfloat16)
        .at[target]
        .set(jnp.repeat(normed, topk, axis=0))
    )
    buffer = buffer.reshape(experts, capacity, width)
    w_gate = gate_weight[0]
    w_up = up_weight[0]
    w_down = down_weight[0]
    rows = lax.all_to_all(buffer, "ep", split_axis=0, concat_axis=0, tiled=True)
    sources, slots, _ = rows.shape
    flat = rows.reshape(-1, width)
    pieces = lax.all_gather((w_gate, w_up), "tp", axis=1, tiled=True)
    gate = jnp.dot(flat, pieces[0], preferred_element_type=jnp.float32)
    upper = jnp.dot(flat, pieces[1], preferred_element_type=jnp.float32)
    hidden = (jax.nn.silu(gate) * upper).astype(jnp.bfloat16)
    result = jnp.dot(
        hidden, lax.all_gather(w_down, "tp", axis=0, tiled=True), preferred_element_type=jnp.float32
    ).astype(jnp.bfloat16)
    returned = lax.all_to_all(
        result.reshape(sources, slots, width), "ep", split_axis=0, concat_axis=0, tiled=True
    )
    picked = returned.reshape(-1, width)[target].astype(jnp.float32).reshape(tok_rows, topk, width)
    return jnp.sum(picked * route_weights[:, :, None], axis=1).astype(jnp.bfloat16)


def solution(mesh):
    placed = (
        P(("ep", "tp"), None),
        P(),
        P(),
        P("ep", None, "tp"),
        P("ep", None, "tp"),
        P("ep", "tp", None),
        P(("ep", "tp"), None),
        P(("ep", "tp"), None),
    )
    return jax.shard_map(
        body, mesh=mesh, in_specs=placed, out_specs=P(("ep", "tp"), None), check_vma=False
    )
```

profile of v0, /device:TPU:0, one launch (start us, length us, event | category | flops | bytes accessed | tf_op | source)
XLA Modules:
  0.0 207.6 jit_solution(8266668216036979915)
XLA Ops:
  6.6 0.7 all-gather.9.cloned.1.call-update
  7.3 0.7 all-gather.7.cloned.1.call-update
  8.4 0.2 convert_reduce_fusion
  8.6 1.2 reduce-window.6
  9.8 0.2 slice_reduce_fusion
  10.0 0.1 eq.25
  10.3 0.1 mul.55
  10.5 0.4 fusion.13
  10.9 0.5 fusion.16
  11.4 1.3 broadcast_in_dim.5
  12.7 2.3 %reshape.104 = bf16[512,2048]{1,0:T(8,128)(2,1)} reshape(bf16[256,2,2048]{2,1,0:T(2,128)(2,1)S(1)} %broadcast_in_dim.5) | data formatting | bytes 4194304 | tf_op jit(solution)/shard_map/reshape | solution.py:25
  15.1 7.3 %scatter_custom_fusion = bf16[1024,2048]{1,0:T(8,128)(2,1)} fusion(s32[512]{0:T(512)S(1)} %bitcast.39, bf16[512,2048]{1,0:T(8,128)(2,1)} %reshape.104, bf16[]{:T(256)} %constant.9.clone.1), kind=kCustom, calls=%fused_computation.19 | custom fusion | bytes 4194816 | tf_op jit(solution)/shard_map/scatter | solution.py:25
  22.5 11.8 %all-to-all-start = ((bf16[64,16,2048]{2,1,0:T(8,128)(2,1)}), bf16[64,16,2048]{2,1,0:T(8,128)(2,1)}, u32[]{:S(2)}, u32[]{:S(2)}) async-start(bf16[64,16,2048]{2,1,0:T(8,128)(2,1)} %bitcast.37), calls=%async_computation | async-start | bytes 8388608 | tf_op jit(solution)/shard_map/all_to_all | solution.py:31
  34.3 0.2 all-gather.11.cloned.1.call-start
  34.5 0.5 all-gather.11.cloned.1.call-update
  35.0 54.5 %all-to-all-done = bf16[64,16,2048]{2,1,0:T(8,128)(2,1)} async-done(((bf16[64,16,2048]{2,1,0:T(8,128)(2,1)}), bf16[64,16,2048]{2,1,0:T(8,128)(2,1)}, u32[]{:S(2)}, u32[]{:S(2)}) %all-to-all-start) | async-done | bytes 4194336 | tf_op jit(solution)/shard_map/all_to_all | solution.py:31
  89.5 9.9 %fusion.2 = f32[1024,1024]{1,0:T(8,128)} fusion(bf16[1024,2048]{1,0:T(8,128)(2,1)} %bitcast.4, bf16[1,2048,1024]{2,1,0:T(8,128)(2,1)} %all-gather.9.cloned.1.call-done), kind=kOutput, calls=%fused_computation.4 | convolution fusion | flops 4294967296 | bytes 12582912 | tf_op jit(solution)/shard_map/dot_general | solution.py:36
  99.4 9.6 %multiply_convert_fusion = bf16[1024,1024]{1,0:T(8,128)(2,1)S(1)} fusion(f32[1024,1024]{1,0:T(8,128)} %fusion.2, bf16[1024,2048]{1,0:T(8,128)(2,1)} %bitcast.4, bf16[1,2048,1024]{2,1,0:T(8,128)(2,1)} %all-gather.7.cloned.1.call-done), kind=kOutput, calls=%fused_computation.9 | convolution fusion | flops 4301258752 | bytes 14680064 | tf_op jit(solution)/shard_map/dot_general | solution.py:35
  109.0 8.2 %fusion.6 = bf16[1024,2048]{1,0:T(8,128)(2,1)} fusion(bf16[1024,1024]{1,0:T(8,128)(2,1)S(1)} %multiply_convert_fusion, bf16[1,1024,2048]{2,1,0:T(8,128)(2,1)} %all-gather.11.cloned.1.call-done), kind=kOutput, calls=%fused_computation.10 | convolution fusion | flops 4297064448 | bytes 10485760 | tf_op jit(solution)/shard_map/dot_general | solution.py:38
  117.2 7.9 %all-to-all-start.1 = ((bf16[64,16,2048]{2,1,0:T(8,128)(2,1)}), bf16[64,16,2048]{2,1,0:T(8,128)(2,1)}, u32[]{:S(2)}, u32[]{:S(2)}) async-start(bf16[64,16,2048]{2,1,0:T(8,128)(2,1)} %bitcast.38), calls=%async_computation.1 | async-start | bytes 8388608 | tf_op jit(solution)/shard_map/all_to_all | solution.py:41
  125.3 54.8 %all-to-all-done.1 = bf16[64,16,2048]{2,1,0:T(8,128)(2,1)} async-done(((bf16[64,16,2048]{2,1,0:T(8,128)(2,1)}), bf16[64,16,2048]{2,1,0:T(8,128)(2,1)}, u32[]{:S(2)}, u32[]{:S(2)}) %all-to-all-start.1) | async-done | bytes 4194336 | tf_op jit(solution)/shard_map/all_to_all | solution.py:41
  180.1 7.1 %gather_fusion = bf16[512,2048]{1,0:T(8,128)(2,1)S(1)} fusion(bf16[1024,2048]{1,0:T(8,128)(2,1)} %bitcast.9, s32[1024]{0:T(1024)S(1)} %pad_clamp_fusion), kind=kCustom, calls=%fused_computation | custom fusion | bytes 4196352 | tf_op jit(solution)/shard_map/gather | solution.py:44
  187.2 4.0 %reshape.91 = f32[256,2,2048]{2,1,0:T(2,128)} reshape(bf16[512,2048]{1,0:T(8,128)(2,1)S(1)} %gather_fusion) | data formatting | bytes 6291456 | tf_op jit(solution)/shard_map/convert_element_type | solution.py:44
  191.2 9.9 %multiply_reduce_fusion = bf16[256,2048]{1,0:T(8,128)(2,1)} fusion(f32[256,2,2048]{2,1,0:T(2,128)} %reshape.91, f32[256,2]{1,0:T(8,128)S(1)} %copy.14), kind=kLoop, calls=%fused_computation.8 | loop fusion | flops 1572864 | bytes 5244928 | tf_op jit(solution)/shard_map/reduce_sum | solution.py:45
  (29 shorter events, 0.9 us)
Async XLA Ops:
  6.5 1.5 copy-start.3
  6.5 1.8 copy-start
  6.5 4.4 %copy-start.1 = (f32[2048]{0:T(1024)S(1)}, f32[2048]{0:T(1024)}, u32[]{:S(2)}) copy-start(f32[2048]{0:T(1024)} %param.10) | copy-start | bytes 24580
  6.5 4.4 %copy-start.2 = (f32[2048]{0:T(1024)S(1)}, f32[2048]{0:T(1024)}, u32[]{:S(2)}) copy-start(f32[2048]{0:T(1024)} %param.9) | copy-start | bytes 24580
  6.5 83.0 %all-gather.9.cloned.1.call-start = ((), (), s32[]{:S(2)}) async-start(), calls=%async_computation.3 | async-start | bytes 6291456 | tf_op jit(solution)/shard_map/all_gather | solution.py:34
  7.3 92.1 %all-gather.7.cloned.1.call-start = ((), (), s32[]{:S(2)}) async-start(), calls=%async_computation.2 | async-start | bytes 6291456 | tf_op jit(solution)/shard_map/all_gather | solution.py:34
  22.5 67.0 %all-to-all-start = ((bf16[64,16,2048]{2,1,0:T(8,128)(2,1)}), bf16[64,16,2048]{2,1,0:T(8,128)(2,1)}, u32[]{:S(2)}, u32[]{:S(2)}) async-start(bf16[64,16,2048]{2,1,0:T(8,128)(2,1)} %bitcast.37), calls=%async_computation | async-start | bytes 8388608 | tf_op jit(solution)/shard_map/all_to_all | solution.py:31
  34.3 74.7 %all-gather.11.cloned.1.call-start = ((), (), s32[]{:S(2)}) async-start(), calls=%async_computation.4 | async-start | bytes 6291456 | tf_op jit(solution)/shard_map/all_gather | solution.py:39
  117.2 7.9 %copy-start.4 = (f32[256,2]{0,1:T(2,128)S(1)}, f32[256,2]{0,1:T(2,128)}, u32[]{:S(2)}) copy-start(f32[256,2]{0,1:T(2,128)} %param.15) | copy-start | bytes 6148
  117.2 62.9 %all-to-all-start.1 = ((bf16[64,16,2048]{2,1,0:T(8,128)(2,1)}), bf16[64,16,2048]{2,1,0:T(8,128)(2,1)}, u32[]{:S(2)}, u32[]{:S(2)}) async-start(bf16[64,16,2048]{2,1,0:T(8,128)(2,1)} %bitcast.38), calls=%async_computation.1 | async-start | bytes 8388608 | tf_op jit(solution)/shard_map/all_to_all | solution.py:41
Sparse Core Ops, SparseCore 0:
  9.0 18.8 all-gather.8
  29.5 17.6 all-gather.6
  48.9 17.6 all-gather.10
where the time goes:
time: 208 us
  waiting for transfers between devices  111 us (53%)
  matrix products  27.7 us (13%)
  local copies, waits for them, and re-layouts  23.1 us (11%)
  starting transfers between devices  20 us (10%)
  between operations  13.3 us (6%)
  other arithmetic  12.4 us (6%)
    all_to_all x1, waiting for transfers between devices, body(): lax.all_to_all(result.reshape(sources, slots, width), 'ep', split_axis=0,...  54.8 us
    all_to_all x1, waiting for transfers between devices, body(): rows = lax.all_to_all(buffer, 'ep', split_axis=0, concat_axis=0, tiled=True)  54.5 us
    all_to_all x1, starting transfers between devices, body(): rows = lax.all_to_all(buffer, 'ep', split_axis=0, concat_axis=0, tiled=True)  11.8 us
    dot_general x1, matrix products, body(): upper = jnp.dot(flat, pieces[1], preferred_element_type=jnp.float32)  9.88 us
    reduce_sum x1, other arithmetic, body(): jnp.sum(picked * route_weights[:, :, None], axis=1).astype(jnp.bfloat16)  9.86 us
    dot_general x1, matrix products, body(): gate = jnp.dot(flat, pieces[0], preferred_element_type=jnp.float32)  9.55 us
    dot_general x1, matrix products, body(): jnp.dot(hidden, lax.all_gather(w_down, 'tp', axis=0, tiled=True), preferr...  8.22 us
    all_to_all x1, starting transfers between devices, body(): lax.all_to_all(result.reshape(sources, slots, width), 'ep', split_axis=0,...  7.93 us
  transfers between devices with their start and end apart: 5, of which 2 were waited for; matrix products, arithmetic and copies ran while one was open for 16% of the time, Pallas kernels for 0%

commit v1 on v0

v1 whole, which is shorter than its diff:
```python
import jax
import jax.numpy as jnp
from jax import lax
from jax.experimental import pallas as pl
from jax.experimental.pallas import tpu as pltpu
from jax.sharding import PartitionSpec as P

BF = jnp.bfloat16
F32 = jnp.float32


def dot(a, b):
    return jnp.dot(a, b, preferred_element_type=F32)


def pack_kernel(experts, capacity, blocks):
    def kernel(tok, gain, bias, ids, ids_t, buf, place, normed, place_t):
        n, width = tok.shape
        rows = experts * capacity // blocks
        step = pl.program_id(0)

        @pl.when(step == 0)
        def _():
            values = tok[...].astype(F32)
            centre = values - jnp.mean(values, axis=-1, keepdims=True)
            spread = jnp.mean(centre * centre, axis=-1, keepdims=True)
            normed[...] = (centre * lax.rsqrt(spread + 1e-05) * gain[...] + bias[...]).astype(BF)
            i = lax.broadcasted_iota(jnp.int32, (n, n), 0)
            j = lax.broadcasted_iota(jnp.int32, (n, n), 1)
            e = lax.broadcasted_iota(jnp.int32, (experts, n), 0)
            one = [(e == ids_t[k : k + 1, :]).astype(F32) for k in range(2)]
            seen = dot((one[0] + one[1]).astype(BF), (i < j).astype(BF))
            for k in range(2):
                slot = jnp.sum(seen * one[k], axis=0, keepdims=True).astype(jnp.int32)
                place_t[k : k + 1, :] = ids_t[k : k + 1, :] * capacity + slot
            e = lax.broadcasted_iota(jnp.int32, (n, experts), 1)
            one = [(e == ids[:, k : k + 1]).astype(F32) for k in range(2)]
            seen = dot((j < i).astype(BF), (one[0] + one[1]).astype(BF))
            for k in range(2):
                slot = jnp.sum(seen * one[k], axis=1, keepdims=True).astype(jnp.int32)
                place[:, k : k + 1] = ids[:, k : k + 1] * capacity + slot

        r = lax.broadcasted_iota(jnp.int32, (rows, n), 0) + step * rows
        hit = (r == place_t[0:1, :]) | (r == place_t[1:2, :])
        buf[...] = dot(jnp.where(hit, 1.0, 0.0).astype(BF), normed[...]).astype(BF)

    return kernel


def pack(tokens, gain, bias, ids, experts, capacity):
    n, width = tokens.shape
    blocks = 4
    whole = lambda s: (0, 0)
    return pl.pallas_call(
        pack_kernel(experts, capacity, blocks),
        grid=(blocks,),
        in_specs=[
            pl.BlockSpec((n, width), whole),
            pl.BlockSpec((1, width), whole),
            pl.BlockSpec((1, width), whole),
            pl.BlockSpec((n, 2), whole),
            pl.BlockSpec((2, n), whole),
        ],
        out_specs=[
            pl.BlockSpec((experts * capacity // blocks, width), lambda s: (s, 0)),
            pl.BlockSpec((n, 2), whole),
        ],
        out_shape=[
            jax.ShapeDtypeStruct((experts * capacity, width), BF),
            jax.ShapeDtypeStruct((n, 2), jnp.int32),
        ],
        scratch_shapes=[pltpu.VMEM((n, width), BF), pltpu.VMEM((2, n), jnp.int32)],
        compiler_params=pltpu.CompilerParams(dimension_semantics=("arbitrary",)),
        name="pack",
    )(tokens, gain.reshape(1, -1), bias.reshape(1, -1), ids, ids.T)


def expert_kernel(x, ga, gb, ua, ub, da, db, out):
    rows = x[...]
    total = None
    for g, u, d in ((ga, ua, da), (gb, ub, db)):
        gate = dot(rows, g[...])
        hidden = (gate / (1.0 + jnp.exp(-gate)) * dot(rows, u[...])).astype(BF)
        part = dot(hidden, d[...])
        total = part if total is None else total + part
    out[...] = total.astype(BF)


def expert(x, weights):
    rows, width = x.shape
    tile = 256
    fixed = [
        pl.BlockSpec(w.shape, lambda s: (0, 0), pipeline_mode=pl.Buffered(1)) for w in weights
    ]
    return pl.pallas_call(
        expert_kernel,
        grid=(rows // tile,),
        in_specs=[pl.BlockSpec((tile, width), lambda s: (s, 0))] + fixed,
        out_specs=pl.BlockSpec((tile, width), lambda s: (s, 0)),
        out_shape=jax.ShapeDtypeStruct((rows, width), BF),
        compiler_params=pltpu.CompilerParams(
            dimension_semantics=("arbitrary",), vmem_limit_bytes=48 * 1024 * 1024
        ),
        name="expert",
    )(x, *weights)


def mix_kernel(ret, place, weight, out, pick):
    n = out.shape[0]
    rows = ret.shape[0]

    @pl.when(pl.program_id(0) == 0)
    def _():
        r = lax.broadcasted_iota(jnp.int32, (n, rows), 1)
        for k in range(2):
            pick[k * n : k * n + n, :] = jnp.where(r == place[:, k : k + 1], 1.0, 0.0).astype(BF)

    picked = dot(pick[...], ret[...])
    out[...] = (picked[:n] * weight[:, 0:1] + picked[n:] * weight[:, 1:2]).astype(BF)


def mix(ret, place, weight):
    rows, width = ret.shape
    n = place.shape[0]
    tile = 512
    return pl.pallas_call(
        mix_kernel,
        grid=(width // tile,),
        in_specs=[
            pl.BlockSpec((rows, tile), lambda s: (0, s)),
            pl.BlockSpec((n, 2), lambda s: (0, 0)),
            pl.BlockSpec((n, 2), lambda s: (0, 0)),
        ],
        out_specs=pl.BlockSpec((n, tile), lambda s: (0, s)),
        out_shape=jax.ShapeDtypeStruct((n, width), BF),
        scratch_shapes=[pltpu.VMEM((2 * n, rows), BF)],
        compiler_params=pltpu.CompilerParams(dimension_semantics=("arbitrary",)),
        name="mix",
    )(ret, place, weight)


def body(
    tokens, norm_gain, norm_bias, gate_weight, up_weight, down_weight, expert_ids, route_weights
):
    tok_rows, width = tokens.shape
    experts = lax.axis_size("ep")
    capacity = max(4 * tok_rows // experts, 4)
    swap = [(0, 1), (1, 0)]
    mine = [gate_weight[0], up_weight[0], down_weight[0]]
    weights = []
    for w in mine:
        weights += [w, lax.ppermute(w, "tp", swap)]
    buffer, place = pack(tokens, norm_gain, norm_bias, expert_ids, experts, capacity)
    rows = lax.all_to_all(
        buffer.reshape(experts, capacity, width), "ep", split_axis=0, concat_axis=0, tiled=True
    )
    result = expert(rows.reshape(-1, width), weights)
    returned = lax.all_to_all(
        result.reshape(experts, capacity, width), "ep", split_axis=0, concat_axis=0, tiled=True
    )
    return mix(returned.reshape(-1, width), place, route_weights)


def solution(mesh):
    placed = (
        P(("ep", "tp"), None),
        P(),
        P(),
        P("ep", None, "tp"),
        P("ep", None, "tp"),
        P("ep", "tp", None),
        P(("ep", "tp"), None),
        P(("ep", "tp"), None),
    )
    return jax.shard_map(
        body, mesh=mesh, in_specs=placed, out_specs=P(("ep", "tp"), None), check_vma=False
    )
```

time: 208 us -> 164 us (0.79)
  Pallas kernels: 0 us -> 30.4 us
  matrix products: 27.7 us -> 0 us
  local copies, waits for them, and re-layouts: 23.1 us -> 5.19 us
  between operations: 13.3 us -> 0.05 us
  other arithmetic: 12.4 us -> 0 us
  waiting for transfers between devices: 111 us -> 108 us
    pallas_call x0 -> x3, Pallas kernels: none -> 30.4 us  [the longest x1 18.9 us: expert(): pl.pallas_call(expert_kernel, grid=(rows // tile,), in_specs=[pl.BlockSpe...]
    dot_general x3 -> x0, matrix products: 27.7 us -> none  [the longest x1 9.88 us: body(): upper = jnp.dot(flat, pieces[1], preferred_element_type=jnp.float32)]
    reduce_sum x4 -> x0, other arithmetic: 10.6 us -> none  [the longest x1 9.86 us: body(): jnp.sum(picked * route_weights[:, :, None], axis=1).astype(jnp.bfloat16)]
    all_to_all x2, waiting for transfers between devices: 109 us -> 99.3 us  [the longest x1 54.4 us: body(): lax.all_to_all(result.reshape(experts, capacity, width), 'ep', split_axis...]
    ppermute x0 -> x3, waiting for transfers between devices: none -> 8.36 us  [body(): weights += [w, lax.ppermute(w, 'tp', swap)]]
    scatter x1 -> x0, local copies, waits for them, and re-layouts: 7.34 us -> none  [body(): buffer = jnp.zeros((experts * capacity, width), jnp.bfloat16).at[target]....]
    gather x1 -> x0, local copies, waits for them, and re-layouts: 7.13 us -> none  [body(): returned.reshape(-1, width)[target].astype(jnp.float32)]
    unnamed x12 -> x10, local copies, waits for them, and re-layouts: 0.28 us -> 5.19 us
  transfers between devices with their start and end apart: 5 -> 5, of which waited for: 2 -> 5; matrix products, arithmetic and copies ran while one was open for 16% -> 0% of each run, Pallas kernels for 0% -> 0%
where the time goes in v1:
time: 164 us
  waiting for transfers between devices  108 us (66%)
  Pallas kernels  30.4 us (19%)
  starting transfers between devices  20.5 us (12%)
  local copies, waits for them, and re-layouts  5.19 us (3%)
    all_to_all x1, waiting for transfers between devices, body(): lax.all_to_all(result.reshape(experts, capacity, width), 'ep', split_axis...  54.4 us
    all_to_all x1, waiting for transfers between devices, body(): lax.all_to_all(buffer.reshape(experts, capacity, width), 'ep', split_axis...  44.9 us
    pallas_call x1, Pallas kernels, expert(): pl.pallas_call(expert_kernel, grid=(rows // tile,), in_specs=[pl.BlockSpe...  18.9 us
    all_to_all x1, starting transfers between devices, body(): lax.all_to_all(buffer.reshape(experts, capacity, width), 'ep', split_axis...  11.9 us
    ppermute x3, waiting for transfers between devices, body(): weights += [w, lax.ppermute(w, 'tp', swap)]  8.36 us
    all_to_all x1, starting transfers between devices, body(): lax.all_to_all(result.reshape(experts, capacity, width), 'ep', split_axis...  7.87 us
    pallas_call x1, Pallas kernels, mix(): pl.pallas_call(mix_kernel, grid=(width // tile,), in_specs=[pl.BlockSpec(...  5.78 us
    pallas_call x1, Pallas kernels, pack(): pl.pallas_call(pack_kernel(experts, capacity, blocks), grid=(blocks,), in...  5.69 us
  transfers between devices with their start and end apart: 5, of which 5 were waited for; matrix products, arithmetic and copies ran while one was open for 0% of the time, Pallas kernels for 0%

profile of v1, /device:TPU:0, one launch (start us, length us, event | category | flops | bytes accessed | tf_op | source)
XLA Modules:
  0.0 163.8 jit_solution(16709167647258476965)
XLA Ops:
  0.0 1.5 copy.9.ids
  1.5 5.7 %pack.1 = (bf16[1024,2048]{1,0:T(8,128)(2,1)}, s32[256,2]{1,0:T(8,128)}) custom-call(bf16[256,2048]{1,0:T(8,128)(2,1)} %tok.1, f32[1,2048]{1,0:T(1,128)} %bitcast.18, f32[1,2048]{1,0:T(1,128)} %bitcast.19, s32[256,2]{1,0:T(8,128)} %copy.9.ids, s32[2,256]{1,0:T(2,128)} %bitcast.20), custom_call_target="tpu_custom_call" | custom-call | tf_op jit(solution)/shard_map/pack/pallas_call | solution.py:54
  7.2 0.0 copy-start
  7.2 11.9 %all-to-all-start = ((bf16[64,16,2048]{2,1,0:T(8,128)(2,1)}), bf16[64,16,2048]{2,1,0:T(8,128)(2,1)}, u32[]{:S(2)}, u32[]{:S(2)}) async-start(bf16[64,16,2048]{2,1,0:T(8,128)(2,1)} %bitcast.13), calls=%async_computation | async-start | bytes 8388608 | tf_op jit(solution)/shard_map/all_to_all | solution.py:154
  19.1 0.0 copy-done
  19.1 0.1 collective-permute-start
  19.2 0.5 collective-permute-start.1
  19.7 0.1 collective-permute-start.2
  19.8 3.6 %collective-permute-done.gb = bf16[2048,512]{1,0:T(8,128)(2,1)S(1)} collective-permute-done((bf16[2048,512]{1,0:T(8,128)(2,1)S(1)}, bf16[2048,512]{1,0:T(8,128)(2,1)S(1)}, u32[]{:S(2)}, u32[]{:S(2)}) %collective-permute-start) | collective-permute-done | bytes 2097184 | tf_op jit(solution)/shard_map/ppermute | solution.py:152
  23.4 0.0 copy-start.1
  23.4 1.3 copy-done.1
  24.7 1.8 %collective-permute-done.1.ub = bf16[2048,512]{1,0:T(8,128)(2,1)} collective-permute-done((bf16[2048,512]{1,0:T(8,128)(2,1)}, bf16[2048,512]{1,0:T(8,128)(2,1)}, u32[]{:S(2)}, u32[]{:S(2)}) %collective-permute-start.1) | collective-permute-done | bytes 2097184 | tf_op jit(solution)/shard_map/ppermute | solution.py:152
  26.5 3.0 %collective-permute-done.2.db = bf16[512,2048]{1,0:T(8,128)(2,1)} collective-permute-done((bf16[512,2048]{1,0:T(8,128)(2,1)}, bf16[512,2048]{1,0:T(8,128)(2,1)}, u32[]{:S(2)}, u32[]{:S(2)}) %collective-permute-start.2) | collective-permute-done | bytes 2097184 | tf_op jit(solution)/shard_map/ppermute | solution.py:152
  29.5 44.9 %all-to-all-done = bf16[64,16,2048]{2,1,0:T(8,128)(2,1)} async-done(((bf16[64,16,2048]{2,1,0:T(8,128)(2,1)}), bf16[64,16,2048]{2,1,0:T(8,128)(2,1)}, u32[]{:S(2)}, u32[]{:S(2)}) %all-to-all-start) | async-done | bytes 4194336 | tf_op jit(solution)/shard_map/all_to_all | solution.py:154
  74.3 0.0 copy-start.2
  74.3 1.6 copy-done.2
  75.9 18.9 %expert.1 = bf16[1024,2048]{1,0:T(8,128)(2,1)} custom-call(bf16[1024,2048]{1,0:T(8,128)(2,1)} %bitcast.4.x, bf16[2048,512]{1,0:T(8,128)(2,1)S(1)} %bitcast.11, bf16[2048,512]{1,0:T(8,128)(2,1)S(1)} %copy-done.2, bf16[2048,512]{1,0:T(8,128)(2,1)} %bitcast.15, bf16[2048,512]{1,0:T(8,128)(2,1)} %collective-permute-done.1.ub, bf16[512,2048]{1,0:T(8,128)(2,1)} %bitcast.17, ...), custom_call_target="tpu_custom_call" | custom-call | tf_op jit(solution)/shard_map/expert/pallas_call | solution.py:95
  94.9 0.0 copy-start.3
  94.9 7.9 %all-to-all-start.1 = ((bf16[64,16,2048]{2,1,0:T(8,128)(2,1)}), bf16[64,16,2048]{2,1,0:T(8,128)(2,1)}, u32[]{:S(2)}, u32[]{:S(2)}) async-start(bf16[64,16,2048]{2,1,0:T(8,128)(2,1)} %bitcast.12), calls=%async_computation.1 | async-start | bytes 8388608 | tf_op jit(solution)/shard_map/all_to_all | solution.py:158
  102.8 0.0 copy-done.3
  102.8 0.8 copy.10.weight
  103.6 54.4 %all-to-all-done.1 = bf16[64,16,2048]{2,1,0:T(8,128)(2,1)} async-done(((bf16[64,16,2048]{2,1,0:T(8,128)(2,1)}), bf16[64,16,2048]{2,1,0:T(8,128)(2,1)}, u32[]{:S(2)}, u32[]{:S(2)}) %all-to-all-start.1) | async-done | bytes 4194336 | tf_op jit(solution)/shard_map/all_to_all | solution.py:158
  158.0 5.8 %mix.1 = bf16[256,2048]{1,0:T(8,128)(2,1)} custom-call(bf16[1024,2048]{1,0:T(8,128)(2,1)} %bitcast.9.ret, s32[256,2]{1,0:T(8,128)} %get-tuple-element.8.place, f32[256,2]{1,0:T(8,128)} %copy.10.weight), custom_call_target="tpu_custom_call" | custom-call | tf_op jit(solution)/shard_map/mix/pallas_call | solution.py:126
Async XLA Ops:
  7.2 11.9 %copy-start = (bf16[1,2048,512]{2,1,0:T(8,128)(2,1)S(1)}, bf16[1,2048,512]{2,1,0:T(8,128)(2,1)}, u32[]{:S(2)}) copy-start(bf16[1,2048,512]{2,1,0:T(8,128)(2,1)} %param.11) | copy-start | bytes 6291460
  7.2 67.2 %all-to-all-start = ((bf16[64,16,2048]{2,1,0:T(8,128)(2,1)}), bf16[64,16,2048]{2,1,0:T(8,128)(2,1)}, u32[]{:S(2)}, u32[]{:S(2)}) async-start(bf16[64,16,2048]{2,1,0:T(8,128)(2,1)} %bitcast.13), calls=%async_computation | async-start | bytes 8388608 | tf_op jit(solution)/shard_map/all_to_all | solution.py:154
  19.1 4.2 %collective-permute-start = (bf16[2048,512]{1,0:T(8,128)(2,1)S(1)}, bf16[2048,512]{1,0:T(8,128)(2,1)S(1)}, u32[]{:S(2)}, u32[]{:S(2)}) collective-permute-start(bf16[2048,512]{1,0:T(8,128)(2,1)S(1)} %bitcast.10), channel_id=1, source_target_pairs={{0,1},{1,0},{2,3},{3,2},{4,5},{5,4},{6,7},{7,6},{8,9},{9,8},{10,11... | collective-permute-start | bytes 6291464 | tf_op jit(solution)/shard_map/ppermute | solution.py:152
  19.2 7.3 %collective-permute-start.1 = (bf16[2048,512]{1,0:T(8,128)(2,1)}, bf16[2048,512]{1,0:T(8,128)(2,1)}, u32[]{:S(2)}, u32[]{:S(2)}) collective-permute-start(bf16[2048,512]{1,0:T(8,128)(2,1)} %bitcast.14), channel_id=1, source_target_pairs={{0,1},{1,0},{2,3},{3,2},{4,5},{5,4},{6,7},{7,6},{8,9},{9,8},{10,11... | collective-permute-start | bytes 6291464 | tf_op jit(solution)/shard_map/ppermute | solution.py:152
  19.7 9.8 %collective-permute-start.2 = (bf16[512,2048]{1,0:T(8,128)(2,1)}, bf16[512,2048]{1,0:T(8,128)(2,1)}, u32[]{:S(2)}, u32[]{:S(2)}) collective-permute-start(bf16[512,2048]{1,0:T(8,128)(2,1)} %bitcast.16), channel_id=1, source_target_pairs={{0,1},{1,0},{2,3},{3,2},{4,5},{5,4},{6,7},{7,6},{8,9},{9,8},{10,11... | collective-permute-start | bytes 6291464 | tf_op jit(solution)/shard_map/ppermute | solution.py:152
  23.4 1.3 copy-start.1
  74.3 1.6 copy-start.2
  94.9 7.9 %copy-start.3 = (f32[256,2]{0,1:T(2,128)S(1)}, f32[256,2]{0,1:T(2,128)}, u32[]{:S(2)}) copy-start(f32[256,2]{0,1:T(2,128)} %param.15) | copy-start | bytes 6148
  94.9 63.1 %all-to-all-start.1 = ((bf16[64,16,2048]{2,1,0:T(8,128)(2,1)}), bf16[64,16,2048]{2,1,0:T(8,128)(2,1)}, u32[]{:S(2)}, u32[]{:S(2)}) async-start(bf16[64,16,2048]{2,1,0:T(8,128)(2,1)} %bitcast.12), calls=%async_computation.1 | async-start | bytes 8388608 | tf_op jit(solution)/shard_map/all_to_all | solution.py:158

commit v2 on v0

v2 whole, which is shorter than its diff:
```python
import jax
import jax.numpy as jnp
from jax import lax
from jax.experimental import pallas as pl
from jax.experimental.pallas import tpu as pltpu
from jax.sharding import PartitionSpec as P


BF = jnp.bfloat16
F32 = jnp.float32


def dot(a, b):
    return jnp.dot(a, b, preferred_element_type=F32)


def place_rows(ids_t, experts, capacity):
    n = ids_t.shape[1]
    i = lax.broadcasted_iota(jnp.int32, (n, n), 0)
    j = lax.broadcasted_iota(jnp.int32, (n, n), 1)
    e = lax.broadcasted_iota(jnp.int32, (experts, n), 0)
    one = [(e == ids_t[k : k + 1, :]).astype(F32) for k in range(2)]
    seen = dot((one[0] + one[1]).astype(BF), (i < j).astype(BF))
    slots = [jnp.sum(seen * o, axis=0, keepdims=True).astype(jnp.int32) for o in one]
    return [ids_t[k : k + 1, :] * capacity + slots[k] for k in range(2)]


def pack_kernel(tok, gain, bias, ids_t, buf):
    n, width = tok.shape
    rows = buf.shape[0]
    experts = rows // CAP
    place = place_rows(ids_t[...], experts, CAP)
    values = tok[...].astype(F32)
    centre = values - jnp.mean(values, axis=-1, keepdims=True)
    spread = jnp.mean(centre * centre, axis=-1, keepdims=True)
    normed = (centre * lax.rsqrt(spread + 1e-05) * gain[...] + bias[...]).astype(BF)
    tile = 256
    for s in range(0, rows, tile):
        r = lax.broadcasted_iota(jnp.int32, (tile, n), 0) + s
        hit = (r == place[0]) | (r == place[1])
        buf[s : s + tile, :] = dot(jnp.where(hit, 1.0, 0.0).astype(BF), normed).astype(BF)


VM = pl.BlockSpec(memory_space=pltpu.VMEM)
CAP = 16
MB = 1024 * 1024


def pack(tokens, gain, bias, ids, rows):
    n, width = tokens.shape
    return pl.pallas_call(
        pack_kernel,
        in_specs=[VM] * 4,
        out_specs=VM,
        out_shape=jax.ShapeDtypeStruct((rows, width), BF),
        compiler_params=pltpu.CompilerParams(vmem_limit_bytes=14 * MB),
        name="pack",
    )(tokens, gain.reshape(1, -1), bias.reshape(1, -1), ids.T)


def expert_kernel(x, ga, gb, ua, ub, da, db, mark, out):
    tile = 256

    def step(i, _):
        at = pl.ds(pl.multiple_of(i * tile, tile), tile)
        rows = x[at, :]
        total = None
        for g, u, d in ((ga, ua, da), (gb, ub, db)):
            gate = dot(rows, g[...])
            hidden = (gate / (1.0 + jnp.exp(-gate)) * dot(rows, u[...])).astype(BF)
            part = dot(hidden, d[...])
            total = part if total is None else total + part
        out[at, :] = total.astype(BF)
        return _

    lax.fori_loop(0, x.shape[0] // tile, step, 0)


def expert(x, weights, mark):
    rows, width = x.shape
    return pl.pallas_call(
        expert_kernel,
        in_specs=[VM] * 8,
        out_specs=VM,
        out_shape=jax.ShapeDtypeStruct((rows, width), BF),
        compiler_params=pltpu.CompilerParams(vmem_limit_bytes=28 * MB),
        name="expert",
    )(x, *weights, mark)


def mix_kernel(ret, ids_t, weight_t, out, side):
    rows = ret.shape[0]
    n, width = out.shape
    place = place_rows(ids_t[...], rows // CAP, CAP)
    side[...] = jnp.zeros(side.shape, F32)
    for k in range(2):
        side[k : k + 1, :] = place[k].astype(F32)
        side[2 + k : 3 + k, :] = weight_t[k : k + 1, :]
    cols = side[...].T
    r = lax.broadcasted_iota(jnp.int32, (n, rows), 1)
    pick = [
        jnp.where(r == cols[:, k : k + 1].astype(jnp.int32), 1.0, 0.0).astype(BF) for k in range(2)
    ]
    tile = 512
    for s in range(0, width, tile):
        part = ret[:, s : s + tile]
        out[:, s : s + tile] = (
            dot(pick[0], part) * cols[:, 2:3] + dot(pick[1], part) * cols[:, 3:4]
        ).astype(BF)


def mix(ret, ids, weight):
    n = ids.shape[0]
    return pl.pallas_call(
        mix_kernel,
        in_specs=[VM] * 3,
        out_specs=VM,
        out_shape=jax.ShapeDtypeStruct((n, ret.shape[1]), BF),
        scratch_shapes=[pltpu.VMEM((8, n), F32)],
        compiler_params=pltpu.CompilerParams(vmem_limit_bytes=14 * MB),
        name="mix",
    )(ret, ids.T, weight.T)


def body(
    tokens, norm_gain, norm_bias, gate_weight, up_weight, down_weight, expert_ids, route_weights
):
    width = tokens.shape[1]
    experts = lax.axis_size("ep")
    swap = [(0, 1), (1, 0)]
    weights = []
    for w in (gate_weight[0], up_weight[0], down_weight[0]):
        weights += [w, lax.ppermute(w, "tp", swap)]
    buffer = pack(tokens, norm_gain, norm_bias, expert_ids, experts * CAP)
    rows = lax.all_to_all(
        buffer.reshape(experts, CAP, width), "ep", split_axis=0, concat_axis=0, tiled=True
    ).reshape(-1, width)
    mark = rows[:16, :128] * 2
    result = expert(rows, weights, mark)
    returned = lax.all_to_all(
        result.reshape(experts, CAP, width), "ep", split_axis=0, concat_axis=0, tiled=True
    )
    return mix(returned.reshape(-1, width), expert_ids, route_weights)


def solution(mesh):
    placed = (
        P(("ep", "tp"), None),
        P(),
        P(),
        P("ep", None, "tp"),
        P("ep", None, "tp"),
        P("ep", "tp", None),
        P(("ep", "tp"), None),
        P(("ep", "tp"), None),
    )
    return jax.shard_map(
        body, mesh=mesh, in_specs=placed, out_specs=P(("ep", "tp"), None), check_vma=False
    )
```

time: 208 us -> 161 us (0.77)
  blocking collectives: 0 us -> 60 us
  waiting for transfers between devices: 111 us -> 54.6 us
  matrix products: 27.7 us -> 0 us
  Pallas kernels: 0 us -> 23.8 us
  local copies, waits for them, and re-layouts: 23.1 us -> 8.45 us
  between operations: 13.3 us -> 0.08 us
  other arithmetic: 12.4 us -> 0.68 us
  starting transfers between devices: 20 us -> 12.6 us
    all_to_all x0 -> x1, blocking collectives: none -> 60 us  [body(): lax.all_to_all(result.reshape(experts, CAP, width), 'ep', split_axis=0, c...]
    all_to_all x2 -> x1, waiting for transfers between devices: 109 us -> 54.5 us  [body(): lax.all_to_all(buffer.reshape(experts, CAP, width), 'ep', split_axis=0, c...]
    dot_general x3 -> x0, matrix products: 27.7 us -> none  [the longest x1 9.88 us: body(): upper = jnp.dot(flat, pieces[1], preferred_element_type=jnp.float32)]
    pallas_call x0 -> x3, Pallas kernels: none -> 23.8 us  [the longest x1 18.1 us: expert(): pl.pallas_call(expert_kernel, in_specs=[VM] * 8, out_specs=VM, out_shape=...]
    reduce_sum x4 -> x0, other arithmetic: 10.6 us -> none  [the longest x1 9.86 us: body(): jnp.sum(picked * route_weights[:, :, None], axis=1).astype(jnp.bfloat16)]
    unnamed x12 -> x20, local copies, waits for them, and re-layouts: 0.28 us -> 8.45 us
    all_to_all x2 -> x1, starting transfers between devices: 19.7 us -> 11.9 us  [body(): lax.all_to_all(buffer.reshape(experts, CAP, width), 'ep', split_axis=0, c...]
    scatter x1 -> x0, local copies, waits for them, and re-layouts: 7.34 us -> none  [body(): buffer = jnp.zeros((experts * capacity, width), jnp.bfloat16).at[target]....]
  transfers between devices with their start and end apart: 5 -> 4, of which waited for: 2 -> 1; matrix products, arithmetic and copies ran while one was open for 16% -> 0% of each run, Pallas kernels for 0% -> 0%
where the time goes in v2:
time: 161 us; the launch traced here: 160 us
  blocking collectives  60 us (37%)
  waiting for transfers between devices  54.6 us (34%)
  Pallas kernels  23.8 us (15%)
  starting transfers between devices  12.6 us (8%)
  local copies, waits for them, and re-layouts  8.45 us (5%)
    all_to_all x1, blocking collectives, body(): lax.all_to_all(result.reshape(experts, CAP, width), 'ep', split_axis=0, c...  60 us
    all_to_all x1, waiting for transfers between devices, body(): lax.all_to_all(buffer.reshape(experts, CAP, width), 'ep', split_axis=0, c...  54.5 us
    pallas_call x1, Pallas kernels, expert(): pl.pallas_call(expert_kernel, in_specs=[VM] * 8, out_specs=VM, out_shape=...  18.1 us
    all_to_all x1, starting transfers between devices, body(): lax.all_to_all(buffer.reshape(experts, CAP, width), 'ep', split_axis=0, c...  11.9 us
    unnamed x20, local copies, waits for them, and re-layouts  8.45 us
    pallas_call x1, Pallas kernels, mix(): pl.pallas_call(mix_kernel, in_specs=[VM] * 3, out_specs=VM, out_shape=jax...  3.81 us
  transfers between devices with their start and end apart: 4, of which 1 were waited for; matrix products, arithmetic and copies ran while one was open for 0% of the time, Pallas kernels for 0%

profile of v2, /device:TPU:0, one launch (start us, length us, event | category | flops | bytes accessed | tf_op | source)
XLA Modules:
  0.0 160.2 jit_solution(12400281324892225557)
XLA Ops:
  0.0 1.2 copy-done.4
  1.2 0.7 copy-done.5
  1.9 0.7 copy-done.6
  2.6 0.7 copy-done.7
  3.3 1.9 %pack.1 = bf16[1024,2048]{1,0:T(8,128)(2,1)S(1)} custom-call(bf16[256,2048]{1,0:T(8,128)(2,1)S(1)} %copy-done.4, f32[1,2048]{1,0:T(1,128)S(1)} %bitcast.20, f32[1,2048]{1,0:T(1,128)S(1)} %bitcast.21, s32[2,256]{1,0:T(2,128)S(1)} %bitcast.22), custom_call_target="tpu_custom_call" | custom-call | tf_op jit(solution)/shard_map/pack/pallas_call | solution.py:51
  5.3 0.0 copy-start
  5.3 2.0 %copy-done = bf16[1024,2048]{1,0:T(8,128)(2,1)} copy-done((bf16[1024,2048]{1,0:T(8,128)(2,1)}, bf16[1024,2048]{1,0:T(8,128)(2,1)S(1)}, u32[]{:S(2)}) %copy-start) | copy-done | bytes 4194328
  7.2 11.9 %all-to-all-start = ((bf16[64,16,2048]{2,1,0:T(8,128)(2,1)}), bf16[64,16,2048]{2,1,0:T(8,128)(2,1)}, u32[]{:S(2)}, u32[]{:S(2)}) async-start(bf16[64,16,2048]{2,1,0:T(8,128)(2,1)} %bitcast.11), calls=%async_computation | async-start | bytes 8388608 | tf_op jit(solution)/shard_map/all_to_all | solution.py:135
  19.2 0.1 collective-permute-start
  19.3 0.5 collective-permute-start.1
  19.8 0.1 collective-permute-start.2
  19.8 54.5 %all-to-all-done = bf16[64,16,2048]{2,1,0:T(8,128)(2,1)} async-done(((bf16[64,16,2048]{2,1,0:T(8,128)(2,1)}), bf16[64,16,2048]{2,1,0:T(8,128)(2,1)}, u32[]{:S(2)}, u32[]{:S(2)}) %all-to-all-start) | async-done | bytes 4194336 | tf_op jit(solution)/shard_map/all_to_all | solution.py:135
  74.4 0.7 slice_multiply_fusion.mark
  75.1 0.0 collective-permute-done.gb
  75.1 0.0 collective-permute-done.1.ub
  75.1 0.0 collective-permute-done.2.db
  75.1 0.0 copy-start.2
  75.1 1.6 copy-done.2
  76.7 1.6 copy-done.3
  78.3 18.1 %expert.1 = bf16[1024,2048]{1,0:T(8,128)(2,1)S(1)} custom-call(bf16[1024,2048]{1,0:T(8,128)(2,1)} %bitcast.4.x, bf16[2048,512]{1,0:T(8,128)(2,1)S(1)} %bitcast.15, bf16[2048,512]{1,0:T(8,128)(2,1)} %collective-permute-done.gb, bf16[2048,512]{1,0:T(8,128)(2,1)S(1)} %bitcast.17, bf16[2048,512]{1,0:T(8,128)(2,1)} %collective-permute-done.1.ub, ...), custom_call_target="tpu_custom_call" | custom-call | tf_op jit(solution)/shard_map/expert/pallas_call | solution.py:81
  96.4 0.0 copy-start.8
  96.4 0.0 copy-start.9
  96.4 60.0 %all_to_all.10 = bf16[64,16,2048]{2,1,0:T(8,128)(2,1)S(1)} all-to-all(bf16[64,16,2048]{2,1,0:T(8,128)(2,1)S(1)} %bitcast.13), channel_id=1, replica_groups=mesh['ep'=64,'tp'=2] {'ep'}, dimensions={0} | all-to-all | bytes 8388608 | tf_op jit(solution)/shard_map/all_to_all | solution.py:140
  156.4 3.8 %mix.1 = bf16[256,2048]{1,0:T(8,128)(2,1)} custom-call(bf16[1024,2048]{1,0:T(8,128)(2,1)S(1)} %bitcast.12, s32[2,256]{1,0:T(2,128)S(1)} %bitcast.23, f32[2,256]{1,0:T(2,128)S(1)} %bitcast.24), custom_call_target="tpu_custom_call" | custom-call | tf_op jit(solution)/shard_map/mix/pallas_call | solution.py:114
  (9 shorter events, 0.0 us)
Async XLA Ops:
  0.0 1.2 copy-start.4
  1.2 0.7 copy-start.5
  1.9 0.7 copy-start.6
  2.6 0.7 copy-start.7
  5.3 2.0 %copy-start = (bf16[1024,2048]{1,0:T(8,128)(2,1)}, bf16[1024,2048]{1,0:T(8,128)(2,1)S(1)}, u32[]{:S(2)}) copy-start(bf16[1024,2048]{1,0:T(8,128)(2,1)S(1)} %pack.1) | copy-start | bytes 12582916
  7.2 11.9 %copy-start.1 = (bf16[1,2048,512]{2,1,0:T(8,128)(2,1)S(1)}, bf16[1,2048,512]{2,1,0:T(8,128)(2,1)}, u32[]{:S(2)}) copy-start(bf16[1,2048,512]{2,1,0:T(8,128)(2,1)} %param.11) | copy-start | bytes 6291460
  7.2 67.2 %all-to-all-start = ((bf16[64,16,2048]{2,1,0:T(8,128)(2,1)}), bf16[64,16,2048]{2,1,0:T(8,128)(2,1)}, u32[]{:S(2)}, u32[]{:S(2)}) async-start(bf16[64,16,2048]{2,1,0:T(8,128)(2,1)} %bitcast.11), calls=%async_computation | async-start | bytes 8388608 | tf_op jit(solution)/shard_map/all_to_all | solution.py:135
  19.2 55.9 %collective-permute-start = (bf16[2048,512]{1,0:T(8,128)(2,1)S(1)}, bf16[2048,512]{1,0:T(8,128)(2,1)}, u32[]{:S(2)}, u32[]{:S(2)}) collective-permute-start(bf16[2048,512]{1,0:T(8,128)(2,1)S(1)} %bitcast.14), channel_id=1, source_target_pairs={{0,1},{1,0},{2,3},{3,2},{4,5},{5,4},{6,7},{7,6},{8,9},{9,8},{10,11... | collective-permute-start | bytes 6291464 | tf_op jit(solution)/shard_map/ppermute | solution.py:133
  19.3 55.8 %collective-permute-start.1 = (bf16[2048,512]{1,0:T(8,128)(2,1)}, bf16[2048,512]{1,0:T(8,128)(2,1)}, u32[]{:S(2)}, u32[]{:S(2)}) collective-permute-start(bf16[2048,512]{1,0:T(8,128)(2,1)} %bitcast.16), channel_id=1, source_target_pairs={{0,1},{1,0},{2,3},{3,2},{4,5},{5,4},{6,7},{7,6},{8,9},{9,8},{10,11... | collective-permute-start | bytes 6291464 | tf_op jit(solution)/shard_map/ppermute | solution.py:133
  19.8 55.3 %collective-permute-start.2 = (bf16[512,2048]{1,0:T(8,128)(2,1)}, bf16[512,2048]{1,0:T(8,128)(2,1)}, u32[]{:S(2)}, u32[]{:S(2)}) collective-permute-start(bf16[512,2048]{1,0:T(8,128)(2,1)} %bitcast.18), channel_id=1, source_target_pairs={{0,1},{1,0},{2,3},{3,2},{4,5},{5,4},{6,7},{7,6},{8,9},{9,8},{10,11... | collective-permute-start | bytes 6291464 | tf_op jit(solution)/shard_map/ppermute | solution.py:133
  75.1 1.6 copy-start.2
  76.7 1.6 copy-start.3
  96.4 60.0 %copy-start.8 = (s32[256,2]{0,1:T(2,128)S(1)}, s32[256,2]{0,1:T(2,128)}, u32[]{:S(2)}) copy-start(s32[256,2]{0,1:T(2,128)} %param.14) | copy-start | bytes 6148
  96.4 60.0 %copy-start.9 = (f32[256,2]{0,1:T(2,128)S(1)}, f32[256,2]{0,1:T(2,128)}, u32[]{:S(2)}) copy-start(f32[256,2]{0,1:T(2,128)} %param.15) | copy-start | bytes 6148

commit v3 on v2

--- a/solution.py
+++ b/solution.py
@@ -25,22 +25,48 @@
     return [ids_t[k : k + 1, :] * capacity + slots[k] for k in range(2)]
 
 
-def pack_kernel(tok, gain, bias, ids_t, buf):
-    n, width = tok.shape
+def stay(a):
+    return pltpu.with_memory_space_constraint(a, pltpu.HBM)
+
+
+def pack_kernel(tok, gain, bias, ids_t, buf, tok_v, gain_v, bias_v, ids_v, normed, sems):
+    n, _ = tok.shape
     rows = buf.shape[0]
-    experts = rows // CAP
-    place = place_rows(ids_t[...], experts, CAP)
-    values = tok[...].astype(F32)
-    centre = values - jnp.mean(values, axis=-1, keepdims=True)
-    spread = jnp.mean(centre * centre, axis=-1, keepdims=True)
-    normed = (centre * lax.rsqrt(spread + 1e-05) * gain[...] + bias[...]).astype(BF)
+    part = n // PARTS
+    small = [
+        pltpu.make_async_copy(src, dst, sems.at[i])
+        for i, (src, dst) in enumerate(((ids_t, ids_v), (gain, gain_v), (bias, bias_v)))
+    ]
+    large = [
+        pltpu.make_async_copy(
+            tok.at[pl.ds(i * part, part)], tok_v.at[pl.ds(i * part, part)], sems.at[3 + i]
+        )
+        for i in range(PARTS)
+    ]
+    for copy in small + large:
+        copy.start()
+    small[0].wait()
+    place = place_rows(ids_v[...], rows // CAP, CAP)
+    small[1].wait()
+    small[2].wait()
+    for i in range(PARTS):
+        large[i].wait()
+        at = pl.ds(i * part, part)
+        values = tok_v[at, :].astype(F32)
+        centre = values - jnp.mean(values, axis=-1, keepdims=True)
+        spread = jnp.mean(centre * centre, axis=-1, keepdims=True)
+        normed[at, :] = (
+            centre * lax.rsqrt(spread + 1e-05) * gain_v[...] + bias_v[...]
+        ).astype(BF)
     tile = 256
     for s in range(0, rows, tile):
         r = lax.broadcasted_iota(jnp.int32, (tile, n), 0) + s
         hit = (r == place[0]) | (r == place[1])
-        buf[s : s + tile, :] = dot(jnp.where(hit, 1.0, 0.0).astype(BF), normed).astype(BF)
+        buf[s : s + tile, :] = dot(jnp.where(hit, 1.0, 0.0).astype(BF), normed[...]).astype(BF)
 
 
+PARTS = 4
+HB = pl.BlockSpec(memory_space=pltpu.HBM)
 VM = pl.BlockSpec(memory_space=pltpu.VMEM)
 CAP = 16
 MB = 1024 * 1024
@@ -50,30 +76,33 @@
     n, width = tokens.shape
     return pl.pallas_call(
         pack_kernel,
-        in_specs=[VM] * 4,
+        in_specs=[HB] * 4,
         out_specs=VM,
         out_shape=jax.ShapeDtypeStruct((rows, width), BF),
+        scratch_shapes=[
+            pltpu.VMEM((n, width), BF),
+            pltpu.VMEM((1, width), F32),
+            pltpu.VMEM((1, width), F32),
+            pltpu.VMEM((2, n), jnp.int32),
+            pltpu.VMEM((n, width), BF),
+            pltpu.SemaphoreType.DMA((3 + PARTS,)),
+        ],
         compiler_params=pltpu.CompilerParams(vmem_limit_bytes=14 * MB),
         name="pack",
-    )(tokens, gain.reshape(1, -1), bias.reshape(1, -1), ids.T)
+    )(*[stay(a) for a in (tokens, gain.reshape(1, -1), bias.reshape(1, -1), ids.T)])
 
 
 def expert_kernel(x, ga, gb, ua, ub, da, db, mark, out):
     tile = 256
-
-    def step(i, _):
-        at = pl.ds(pl.multiple_of(i * tile, tile), tile)
-        rows = x[at, :]
+    for s in range(0, x.shape[0], tile):
+        rows = x[s : s + tile, :]
         total = None
         for g, u, d in ((ga, ua, da), (gb, ub, db)):
             gate = dot(rows, g[...])
             hidden = (gate / (1.0 + jnp.exp(-gate)) * dot(rows, u[...])).astype(BF)
             part = dot(hidden, d[...])
             total = part if total is None else total + part
-        out[at, :] = total.astype(BF)
-        return _
-
-    lax.fori_loop(0, x.shape[0] // tile, step, 0)
+        out[s : s + tile, :] = total.astype(BF)
 
 
 def expert(x, weights, mark):
@@ -88,7 +117,7 @@
     )(x, *weights, mark)
 
 
-def mix_kernel(ret, ids_t, weight_t, out, side):
+def mix_kernel(ret, ids_t, weight_t, out, side, done, sems):
     rows = ret.shape[0]
     n, width = out.shape
     place = place_rows(ids_t[...], rows // CAP, CAP)
@@ -101,12 +130,19 @@
     pick = [
         jnp.where(r == cols[:, k : k + 1].astype(jnp.int32), 1.0, 0.0).astype(BF) for k in range(2)
     ]
-    tile = 512
-    for s in range(0, width, tile):
-        part = ret[:, s : s + tile]
-        out[:, s : s + tile] = (
+    for i in range(TILES):
+        at = pl.ds(i * (width // TILES), width // TILES)
+        part = ret[:, at]
+        done[:, at] = (
             dot(pick[0], part) * cols[:, 2:3] + dot(pick[1], part) * cols[:, 3:4]
         ).astype(BF)
+        pltpu.make_async_copy(done.at[:, at], out.at[:, at], sems.at[i]).start()
+    for i in range(TILES):
+        at = pl.ds(i * (width // TILES), width // TILES)
+        pltpu.make_async_copy(done.at[:, at], out.at[:, at], sems.at[i]).wait()
+
+
+TILES = 4
 
 
 def mix(ret, ids, weight):
@@ -114,9 +150,13 @@
     return pl.pallas_call(
         mix_kernel,
         in_specs=[VM] * 3,
-        out_specs=VM,
+        out_specs=HB,
         out_shape=jax.ShapeDtypeStruct((n, ret.shape[1]), BF),
-        scratch_shapes=[pltpu.VMEM((8, n), F32)],
+        scratch_shapes=[
+            pltpu.VMEM((8, n), F32),
+            pltpu.VMEM((n, ret.shape[1]), BF),
+            pltpu.SemaphoreType.DMA((TILES,)),
+        ],
         compiler_params=pltpu.CompilerParams(vmem_limit_bytes=14 * MB),
         name="mix",
     )(ret, ids.T, weight.T)

time: 161 us -> 158 us (0.981)
  local copies, waits for them, and re-layouts: 8.45 us -> 5.16 us
    unnamed x20 -> x12, local copies, waits for them, and re-layouts: 8.45 us -> 5.16 us
where the time goes in v3:
time: 158 us
  blocking collectives  60 us (38%)
  waiting for transfers between devices  54.6 us (35%)
  Pallas kernels  24.5 us (16%)
  starting transfers between devices  12.6 us (8%)
  local copies, waits for them, and re-layouts  5.16 us (3%)
    all_to_all x1, blocking collectives, body(): lax.all_to_all(result.reshape(experts, CAP, width), 'ep', split_axis=0, c...  60 us
    all_to_all x1, waiting for transfers between devices, body(): lax.all_to_all(buffer.reshape(experts, CAP, width), 'ep', split_axis=0, c...  54.6 us
    pallas_call x1, Pallas kernels, expert(): pl.pallas_call(expert_kernel, in_specs=[VM] * 8, out_specs=VM, out_shape=...  17.5 us
    all_to_all x1, starting transfers between devices, body(): lax.all_to_all(buffer.reshape(experts, CAP, width), 'ep', split_axis=0, c...  11.9 us
    unnamed x12, local copies, waits for them, and re-layouts  5.16 us
    pallas_call x1, Pallas kernels, mix(): pl.pallas_call(mix_kernel, in_specs=[VM] * 3, out_specs=HB, out_shape=jax...  3.56 us
    pallas_call x1, Pallas kernels, pack(): pl.pallas_call(pack_kernel, in_specs=[HB] * 4, out_specs=VM, out_shape=ja...  3.41 us
  transfers between devices with their start and end apart: 4, of which 1 were waited for; matrix products, arithmetic and copies ran while one was open for 0% of the time, Pallas kernels for 0%

profile of v3, /device:TPU:0, one launch (start us, length us, event | category | flops | bytes accessed | tf_op | source)
XLA Modules:
  0.0 157.8 jit_solution(11446918796202833456)
XLA Ops:
  0.0 3.4 %pack.1 = bf16[1024,2048]{1,0:T(8,128)(2,1)S(1)} custom-call(bf16[256,2048]{1,0:T(8,128)(2,1)} %tok.1, f32[1,2048]{1,0:T(1,128)} %bitcast.23, f32[1,2048]{1,0:T(1,128)} %bitcast.24, s32[2,256]{1,0:T(2,128)} %bitcast.20), custom_call_target="tpu_custom_call" | custom-call | tf_op jit(solution)/shard_map/pack/pallas_call | solution.py:77
  3.4 0.0 copy-start
  3.4 2.0 %copy-done = bf16[1024,2048]{1,0:T(8,128)(2,1)} copy-done((bf16[1024,2048]{1,0:T(8,128)(2,1)}, bf16[1024,2048]{1,0:T(8,128)(2,1)S(1)}, u32[]{:S(2)}) %copy-start) | copy-done | bytes 4194328
  5.4 0.0 copy-start.1
  5.4 11.9 %all-to-all-start = ((bf16[64,16,2048]{2,1,0:T(8,128)(2,1)}), bf16[64,16,2048]{2,1,0:T(8,128)(2,1)}, u32[]{:S(2)}, u32[]{:S(2)}) async-start(bf16[64,16,2048]{2,1,0:T(8,128)(2,1)} %bitcast.11), calls=%async_computation | async-start | bytes 8388608 | tf_op jit(solution)/shard_map/all_to_all | solution.py:175
  17.3 0.0 copy-done.1
  17.3 0.1 collective-permute-start
  17.4 0.5 collective-permute-start.1
  17.9 0.1 collective-permute-start.2
  18.0 54.6 %all-to-all-done = bf16[64,16,2048]{2,1,0:T(8,128)(2,1)} async-done(((bf16[64,16,2048]{2,1,0:T(8,128)(2,1)}), bf16[64,16,2048]{2,1,0:T(8,128)(2,1)}, u32[]{:S(2)}, u32[]{:S(2)}) %all-to-all-start) | async-done | bytes 4194336 | tf_op jit(solution)/shard_map/all_to_all | solution.py:175
  72.6 0.7 slice_multiply_fusion.mark
  73.2 0.0 collective-permute-done.gb
  73.3 0.0 collective-permute-done.1.ub
  73.3 0.0 collective-permute-done.2.db
  73.3 0.0 copy-start.2
  73.3 1.6 %copy-done.2 = bf16[1,2048,512]{2,1,0:T(8,128)(2,1)S(1)} copy-done((bf16[1,2048,512]{2,1,0:T(8,128)(2,1)S(1)}, bf16[1,2048,512]{2,1,0:T(8,128)(2,1)}, u32[]{:S(2)}) %copy-start.2) | copy-done | bytes 2097176
  74.9 1.6 %copy-done.3 = bf16[1,512,2048]{2,1,0:T(8,128)(2,1)S(1)} copy-done((bf16[1,512,2048]{2,1,0:T(8,128)(2,1)S(1)}, bf16[1,512,2048]{2,1,0:T(8,128)(2,1)}, u32[]{:S(2)}) %copy-start.3) | copy-done | bytes 2097176
  76.4 17.5 %expert.1 = bf16[1024,2048]{1,0:T(8,128)(2,1)S(1)} custom-call(bf16[1024,2048]{1,0:T(8,128)(2,1)} %bitcast.4.x, bf16[2048,512]{1,0:T(8,128)(2,1)S(1)} %bitcast.15, bf16[2048,512]{1,0:T(8,128)(2,1)} %collective-permute-done.gb, bf16[2048,512]{1,0:T(8,128)(2,1)S(1)} %bitcast.17, bf16[2048,512]{1,0:T(8,128)(2,1)} %collective-permute-done.1.ub, ...), custom_call_target="tpu_custom_call" | custom-call | tf_op jit(solution)/shard_map/expert/pallas_call | solution.py:110
  94.0 0.0 copy-start.4
  94.0 0.0 copy-start.5
  94.0 60.0 %all_to_all.10 = bf16[64,16,2048]{2,1,0:T(8,128)(2,1)S(1)} all-to-all(bf16[64,16,2048]{2,1,0:T(8,128)(2,1)S(1)} %bitcast.13), channel_id=1, replica_groups=mesh['ep'=64,'tp'=2] {'ep'}, dimensions={0} | all-to-all | bytes 8388608 | tf_op jit(solution)/shard_map/all_to_all | solution.py:180
  154.0 0.0 copy-done.4
  154.0 0.0 copy-done.5
  154.0 3.6 %mix.1 = bf16[256,2048]{1,0:T(8,128)(2,1)} custom-call(bf16[1024,2048]{1,0:T(8,128)(2,1)S(1)} %bitcast.12, s32[2,256]{1,0:T(2,128)S(1)} %bitcast.21, f32[2,256]{1,0:T(2,128)S(1)} %bitcast.22), custom_call_target="tpu_custom_call" | custom-call | tf_op jit(solution)/shard_map/mix/pallas_call | solution.py:150
  (1 shorter events, 0.0 us)
Async XLA Ops:
  3.4 2.0 %copy-start = (bf16[1024,2048]{1,0:T(8,128)(2,1)}, bf16[1024,2048]{1,0:T(8,128)(2,1)S(1)}, u32[]{:S(2)}) copy-start(bf16[1024,2048]{1,0:T(8,128)(2,1)S(1)} %pack.1) | copy-start | bytes 12582916
  5.4 11.9 %copy-start.1 = (bf16[1,2048,512]{2,1,0:T(8,128)(2,1)S(1)}, bf16[1,2048,512]{2,1,0:T(8,128)(2,1)}, u32[]{:S(2)}) copy-start(bf16[1,2048,512]{2,1,0:T(8,128)(2,1)} %param.11) | copy-start | bytes 6291460
  5.4 67.2 %all-to-all-start = ((bf16[64,16,2048]{2,1,0:T(8,128)(2,1)}), bf16[64,16,2048]{2,1,0:T(8,128)(2,1)}, u32[]{:S(2)}, u32[]{:S(2)}) async-start(bf16[64,16,2048]{2,1,0:T(8,128)(2,1)} %bitcast.11), calls=%async_computation | async-start | bytes 8388608 | tf_op jit(solution)/shard_map/all_to_all | solution.py:175
  17.3 55.9 %collective-permute-start = (bf16[2048,512]{1,0:T(8,128)(2,1)S(1)}, bf16[2048,512]{1,0:T(8,128)(2,1)}, u32[]{:S(2)}, u32[]{:S(2)}) collective-permute-start(bf16[2048,512]{1,0:T(8,128)(2,1)S(1)} %bitcast.14), channel_id=1, source_target_pairs={{0,1},{1,0},{2,3},{3,2},{4,5},{5,4},{6,7},{7,6},{8,9},{9,8},{10,11... | collective-permute-start | bytes 6291464 | tf_op jit(solution)/shard_map/ppermute | solution.py:173
  17.4 55.8 %collective-permute-start.1 = (bf16[2048,512]{1,0:T(8,128)(2,1)}, bf16[2048,512]{1,0:T(8,128)(2,1)}, u32[]{:S(2)}, u32[]{:S(2)}) collective-permute-start(bf16[2048,512]{1,0:T(8,128)(2,1)} %bitcast.16), channel_id=1, source_target_pairs={{0,1},{1,0},{2,3},{3,2},{4,5},{5,4},{6,7},{7,6},{8,9},{9,8},{10,11... | collective-permute-start | bytes 6291464 | tf_op jit(solution)/shard_map/ppermute | solution.py:173
  17.9 55.3 %collective-permute-start.2 = (bf16[512,2048]{1,0:T(8,128)(2,1)}, bf16[512,2048]{1,0:T(8,128)(2,1)}, u32[]{:S(2)}, u32[]{:S(2)}) collective-permute-start(bf16[512,2048]{1,0:T(8,128)(2,1)} %bitcast.18), channel_id=1, source_target_pairs={{0,1},{1,0},{2,3},{3,2},{4,5},{5,4},{6,7},{7,6},{8,9},{9,8},{10,11... | collective-permute-start | bytes 6291464 | tf_op jit(solution)/shard_map/ppermute | solution.py:173
  73.3 1.6 %copy-start.2 = (bf16[1,2048,512]{2,1,0:T(8,128)(2,1)S(1)}, bf16[1,2048,512]{2,1,0:T(8,128)(2,1)}, u32[]{:S(2)}) copy-start(bf16[1,2048,512]{2,1,0:T(8,128)(2,1)} %param.12) | copy-start | bytes 6291460
  74.9 1.6 %copy-start.3 = (bf16[1,512,2048]{2,1,0:T(8,128)(2,1)S(1)}, bf16[1,512,2048]{2,1,0:T(8,128)(2,1)}, u32[]{:S(2)}) copy-start(bf16[1,512,2048]{2,1,0:T(8,128)(2,1)} %param.13) | copy-start | bytes 6291460
  94.0 60.0 %copy-start.4 = (s32[256,2]{0,1:T(2,128)S(1)}, s32[256,2]{0,1:T(2,128)}, u32[]{:S(2)}) copy-start(s32[256,2]{0,1:T(2,128)} %param.14) | copy-start | bytes 6148
  94.0 60.0 %copy-start.5 = (f32[256,2]{0,1:T(2,128)S(1)}, f32[256,2]{0,1:T(2,128)}, u32[]{:S(2)}) copy-start(f32[256,2]{0,1:T(2,128)} %param.15) | copy-start | bytes 6148

commit v4 on v3

--- a/solution.py
+++ b/solution.py
@@ -29,7 +29,7 @@
     return pltpu.with_memory_space_constraint(a, pltpu.HBM)
 
 
-def pack_kernel(tok, gain, bias, ids_t, buf, tok_v, gain_v, bias_v, ids_v, normed, sems):
+def pack_kernel(tok, gain, bias, ids_t, buf, tok_v, gain_v, bias_v, ids_v, normed, ticks, sems):
     n, _ = tok.shape
     rows = buf.shape[0]
     part = n // PARTS
@@ -45,6 +45,13 @@
     ]
     for copy in small + large:
         copy.start()
+    ticks[0] = 0
+
+    def tick(i, carry):
+        ticks[0] = ticks[0] + i
+        return carry
+
+    lax.fori_loop(0, lax.axis_index("tp") * HOLD, tick, 0)
     small[0].wait()
     place = place_rows(ids_v[...], rows // CAP, CAP)
     small[1].wait()
@@ -66,6 +73,7 @@
 
 
 PARTS = 4
+HOLD = 3050
 HB = pl.BlockSpec(memory_space=pltpu.HBM)
 VM = pl.BlockSpec(memory_space=pltpu.VMEM)
 CAP = 16
@@ -85,6 +93,7 @@
             pltpu.VMEM((1, width), F32),
             pltpu.VMEM((2, n), jnp.int32),
             pltpu.VMEM((n, width), BF),
+            pltpu.SMEM((1,), jnp.int32),
             pltpu.SemaphoreType.DMA((3 + PARTS,)),
         ],
         compiler_params=pltpu.CompilerParams(vmem_limit_bytes=14 * MB),

time: 158 us -> 145 us (0.918)
  the two profiles are of different devices: /device:TPU:0 before, /device:TPU:1 now
where the time goes in v4:
time: 145 us
  Pallas kernels  49 us (34%)
  blocking collectives  46.8 us (32%)
  waiting for transfers between devices  30.2 us (21%)
  starting transfers between devices  13 us (9%)
  local copies, waits for them, and re-layouts  5.16 us (4%)
    all_to_all x1, blocking collectives, body(): lax.all_to_all(result.reshape(experts, CAP, width), 'ep', split_axis=0, c...  46.8 us
    all_to_all x1, waiting for transfers between devices, body(): lax.all_to_all(buffer.reshape(experts, CAP, width), 'ep', split_axis=0, c...  30.1 us
    pallas_call x1, Pallas kernels, pack(): pl.pallas_call(pack_kernel, in_specs=[HB] * 4, out_specs=VM, out_shape=ja...  27.9 us
    pallas_call x1, Pallas kernels, expert(): pl.pallas_call(expert_kernel, in_specs=[VM] * 8, out_specs=VM, out_shape=...  17.6 us
    all_to_all x1, starting transfers between devices, body(): lax.all_to_all(buffer.reshape(experts, CAP, width), 'ep', split_axis=0, c...  12.3 us
    unnamed x12, local copies, waits for them, and re-layouts  5.16 us
    pallas_call x1, Pallas kernels, mix(): pl.pallas_call(mix_kernel, in_specs=[VM] * 3, out_specs=HB, out_shape=jax...  3.58 us
  transfers between devices with their start and end apart: 4, of which 1 were waited for; matrix products, arithmetic and copies ran while one was open for 0% of the time, Pallas kernels for 0%

profile of v4, /device:TPU:1, one launch (start us, length us, event | category | flops | bytes accessed | tf_op | source)
XLA Modules:
  0.0 145.1 jit_solution(1410603827232917360)
XLA Ops:
  0.0 27.9 %pack.1 = bf16[1024,2048]{1,0:T(8,128)(2,1)S(1)} custom-call(bf16[256,2048]{1,0:T(8,128)(2,1)} %tok.1, f32[1,2048]{1,0:T(1,128)} %bitcast.23, f32[1,2048]{1,0:T(1,128)} %bitcast.24, s32[2,256]{1,0:T(2,128)} %bitcast.20), custom_call_target="tpu_custom_call" | custom-call | tf_op jit(solution)/shard_map/pack/pallas_call | solution.py:85
  27.9 0.0 copy-start
  27.9 2.0 %copy-done = bf16[1024,2048]{1,0:T(8,128)(2,1)} copy-done((bf16[1024,2048]{1,0:T(8,128)(2,1)}, bf16[1024,2048]{1,0:T(8,128)(2,1)S(1)}, u32[]{:S(2)}) %copy-start) | copy-done | bytes 4194328
  29.8 0.0 copy-start.1
  29.8 12.3 %all-to-all-start = ((bf16[64,16,2048]{2,1,0:T(8,128)(2,1)}), bf16[64,16,2048]{2,1,0:T(8,128)(2,1)}, u32[]{:S(2)}, u32[]{:S(2)}) async-start(bf16[64,16,2048]{2,1,0:T(8,128)(2,1)} %bitcast.11), calls=%async_computation | async-start | bytes 8388608 | tf_op jit(solution)/shard_map/all_to_all | solution.py:184
  42.2 0.0 copy-done.1
  42.2 0.1 collective-permute-start
  42.3 0.5 collective-permute-start.1
  42.8 0.1 collective-permute-start.2
  42.9 30.1 %all-to-all-done = bf16[64,16,2048]{2,1,0:T(8,128)(2,1)} async-done(((bf16[64,16,2048]{2,1,0:T(8,128)(2,1)}), bf16[64,16,2048]{2,1,0:T(8,128)(2,1)}, u32[]{:S(2)}, u32[]{:S(2)}) %all-to-all-start) | async-done | bytes 4194336 | tf_op jit(solution)/shard_map/all_to_all | solution.py:184
  73.1 0.7 slice_multiply_fusion.mark
  73.7 0.0 collective-permute-done.gb
  73.7 0.0 collective-permute-done.1.ub
  73.7 0.0 collective-permute-done.2.db
  73.7 0.0 copy-start.2
  73.8 1.6 %copy-done.2 = bf16[1,2048,512]{2,1,0:T(8,128)(2,1)S(1)} copy-done((bf16[1,2048,512]{2,1,0:T(8,128)(2,1)S(1)}, bf16[1,2048,512]{2,1,0:T(8,128)(2,1)}, u32[]{:S(2)}) %copy-start.2) | copy-done | bytes 2097176
  75.3 1.6 %copy-done.3 = bf16[1,512,2048]{2,1,0:T(8,128)(2,1)S(1)} copy-done((bf16[1,512,2048]{2,1,0:T(8,128)(2,1)S(1)}, bf16[1,512,2048]{2,1,0:T(8,128)(2,1)}, u32[]{:S(2)}) %copy-start.3) | copy-done | bytes 2097176
  76.9 17.6 %expert.1 = bf16[1024,2048]{1,0:T(8,128)(2,1)S(1)} custom-call(bf16[1024,2048]{1,0:T(8,128)(2,1)} %bitcast.4.x, bf16[2048,512]{1,0:T(8,128)(2,1)S(1)} %bitcast.15, bf16[2048,512]{1,0:T(8,128)(2,1)} %collective-permute-done.gb, bf16[2048,512]{1,0:T(8,128)(2,1)S(1)} %bitcast.17, bf16[2048,512]{1,0:T(8,128)(2,1)} %collective-permute-done.1.ub, ...), custom_call_target="tpu_custom_call" | custom-call | tf_op jit(solution)/shard_map/expert/pallas_call | solution.py:119
  94.5 0.0 copy-start.4
  94.5 0.0 copy-start.5
  94.5 46.8 %all_to_all.10 = bf16[64,16,2048]{2,1,0:T(8,128)(2,1)S(1)} all-to-all(bf16[64,16,2048]{2,1,0:T(8,128)(2,1)S(1)} %bitcast.13), channel_id=1, replica_groups=mesh['ep'=64,'tp'=2] {'ep'}, dimensions={0} | all-to-all | bytes 8388608 | tf_op jit(solution)/shard_map/all_to_all | solution.py:189
  141.3 0.0 copy-done.4
  141.3 0.0 copy-done.5
  141.3 3.6 %mix.1 = bf16[256,2048]{1,0:T(8,128)(2,1)} custom-call(bf16[1024,2048]{1,0:T(8,128)(2,1)S(1)} %bitcast.12, s32[2,256]{1,0:T(2,128)S(1)} %bitcast.21, f32[2,256]{1,0:T(2,128)S(1)} %bitcast.22), custom_call_target="tpu_custom_call" | custom-call | tf_op jit(solution)/shard_map/mix/pallas_call | solution.py:159
  (1 shorter events, 0.0 us)
Async XLA Ops:
  27.9 2.0 %copy-start = (bf16[1024,2048]{1,0:T(8,128)(2,1)}, bf16[1024,2048]{1,0:T(8,128)(2,1)S(1)}, u32[]{:S(2)}) copy-start(bf16[1024,2048]{1,0:T(8,128)(2,1)S(1)} %pack.1) | copy-start | bytes 12582916
  29.8 12.4 %copy-start.1 = (bf16[1,2048,512]{2,1,0:T(8,128)(2,1)S(1)}, bf16[1,2048,512]{2,1,0:T(8,128)(2,1)}, u32[]{:S(2)}) copy-start(bf16[1,2048,512]{2,1,0:T(8,128)(2,1)} %param.11) | copy-start | bytes 6291460
  29.8 43.2 %all-to-all-start = ((bf16[64,16,2048]{2,1,0:T(8,128)(2,1)}), bf16[64,16,2048]{2,1,0:T(8,128)(2,1)}, u32[]{:S(2)}, u32[]{:S(2)}) async-start(bf16[64,16,2048]{2,1,0:T(8,128)(2,1)} %bitcast.11), calls=%async_computation | async-start | bytes 8388608 | tf_op jit(solution)/shard_map/all_to_all | solution.py:184
  42.2 31.5 %collective-permute-start = (bf16[2048,512]{1,0:T(8,128)(2,1)S(1)}, bf16[2048,512]{1,0:T(8,128)(2,1)}, u32[]{:S(2)}, u32[]{:S(2)}) collective-permute-start(bf16[2048,512]{1,0:T(8,128)(2,1)S(1)} %bitcast.14), channel_id=1, source_target_pairs={{0,1},{1,0},{2,3},{3,2},{4,5},{5,4},{6,7},{7,6},{8,9},{9,8},{10,11... | collective-permute-start | bytes 6291464 | tf_op jit(solution)/shard_map/ppermute | solution.py:182
  42.3 31.4 %collective-permute-start.1 = (bf16[2048,512]{1,0:T(8,128)(2,1)}, bf16[2048,512]{1,0:T(8,128)(2,1)}, u32[]{:S(2)}, u32[]{:S(2)}) collective-permute-start(bf16[2048,512]{1,0:T(8,128)(2,1)} %bitcast.16), channel_id=1, source_target_pairs={{0,1},{1,0},{2,3},{3,2},{4,5},{5,4},{6,7},{7,6},{8,9},{9,8},{10,11... | collective-permute-start | bytes 6291464 | tf_op jit(solution)/shard_map/ppermute | solution.py:182
  42.8 30.9 %collective-permute-start.2 = (bf16[512,2048]{1,0:T(8,128)(2,1)}, bf16[512,2048]{1,0:T(8,128)(2,1)}, u32[]{:S(2)}, u32[]{:S(2)}) collective-permute-start(bf16[512,2048]{1,0:T(8,128)(2,1)} %bitcast.18), channel_id=1, source_target_pairs={{0,1},{1,0},{2,3},{3,2},{4,5},{5,4},{6,7},{7,6},{8,9},{9,8},{10,11... | collective-permute-start | bytes 6291464 | tf_op jit(solution)/shard_map/ppermute | solution.py:182
  73.7 1.6 %copy-start.2 = (bf16[1,2048,512]{2,1,0:T(8,128)(2,1)S(1)}, bf16[1,2048,512]{2,1,0:T(8,128)(2,1)}, u32[]{:S(2)}) copy-start(bf16[1,2048,512]{2,1,0:T(8,128)(2,1)} %param.12) | copy-start | bytes 6291460
  75.3 1.6 %copy-start.3 = (bf16[1,512,2048]{2,1,0:T(8,128)(2,1)S(1)}, bf16[1,512,2048]{2,1,0:T(8,128)(2,1)}, u32[]{:S(2)}) copy-start(bf16[1,512,2048]{2,1,0:T(8,128)(2,1)} %param.13) | copy-start | bytes 6291460
  94.5 46.8 %copy-start.4 = (s32[256,2]{0,1:T(2,128)S(1)}, s32[256,2]{0,1:T(2,128)}, u32[]{:S(2)}) copy-start(s32[256,2]{0,1:T(2,128)} %param.14) | copy-start | bytes 6148
  94.5 46.8 %copy-start.5 = (f32[256,2]{0,1:T(2,128)S(1)}, f32[256,2]{0,1:T(2,128)}, u32[]{:S(2)}) copy-start(f32[256,2]{0,1:T(2,128)} %param.15) | copy-start | bytes 6148

commit v5 on v3

--- a/solution.py
+++ b/solution.py
@@ -25,28 +25,59 @@
     return [ids_t[k : k + 1, :] * capacity + slots[k] for k in range(2)]
 
 
+def picks(place, weight_t, side, pick):
+    side[...] = jnp.zeros(side.shape, F32)
+    for k in range(2):
+        side[k : k + 1, :] = place[k].astype(F32)
+        side[2 + k : 3 + k, :] = weight_t[k : k + 1, :]
+    cols = side[...].T
+    r = lax.broadcasted_iota(jnp.int32, pick.shape, 1)
+    hit = [r == cols[:, k : k + 1].astype(jnp.int32) for k in range(2)]
+    pick[...] = jnp.where(
+        hit[0], cols[:, 2:3], jnp.where(hit[1], cols[:, 3:4], 0.0)
+    ).astype(BF)
+
+
 def stay(a):
     return pltpu.with_memory_space_constraint(a, pltpu.HBM)
 
 
-def pack_kernel(tok, gain, bias, ids_t, buf, tok_v, gain_v, bias_v, ids_v, normed, sems):
+def pack_kernel(
+    tok, gain, bias, ids_t, weight_t, buf, pick,
+    tok_v, gain_v, bias_v, ids_v, weight_v, normed, side, ticks, sems,
+):
     n, _ = tok.shape
     rows = buf.shape[0]
     part = n // PARTS
     small = [
         pltpu.make_async_copy(src, dst, sems.at[i])
-        for i, (src, dst) in enumerate(((ids_t, ids_v), (gain, gain_v), (bias, bias_v)))
+        for i, (src, dst) in enumerate(
+            ((ids_t, ids_v), (gain, gain_v), (bias, bias_v), (weight_t, weight_v))
+        )
     ]
     large = [
         pltpu.make_async_copy(
-            tok.at[pl.ds(i * part, part)], tok_v.at[pl.ds(i * part, part)], sems.at[3 + i]
+            tok.at[pl.ds(i * part, part)], tok_v.at[pl.ds(i * part, part)], sems.at[4 + i]
         )
         for i in range(PARTS)
     ]
     for copy in small + large:
         copy.start()
     small[0].wait()
+    small[3].wait()
     place = place_rows(ids_v[...], rows // CAP, CAP)
+
+    @pl.when(lax.axis_index("tp") == LAST)
+    def _():
+        picks(place, weight_v, side, pick)
+        ticks[0] = 0
+
+        def tick(i, carry):
+            ticks[0] = ticks[0] + i
+            return carry
+
+        lax.fori_loop(0, HOLD, tick, 0)
+
     small[1].wait()
     small[2].wait()
     for i in range(PARTS):
@@ -66,30 +97,38 @@
 
 
 PARTS = 4
+HOLD = 2900
+LAST = 1
 HB = pl.BlockSpec(memory_space=pltpu.HBM)
 VM = pl.BlockSpec(memory_space=pltpu.VMEM)
 CAP = 16
 MB = 1024 * 1024
 
 
-def pack(tokens, gain, bias, ids, rows):
+def pack(tokens, gain, bias, ids, weight, rows):
     n, width = tokens.shape
     return pl.pallas_call(
         pack_kernel,
-        in_specs=[HB] * 4,
-        out_specs=VM,
-        out_shape=jax.ShapeDtypeStruct((rows, width), BF),
+        in_specs=[HB] * 5,
+        out_specs=[VM] * 2,
+        out_shape=[
+            jax.ShapeDtypeStruct((rows, width), BF),
+            jax.ShapeDtypeStruct((n, rows), BF),
+        ],
         scratch_shapes=[
             pltpu.VMEM((n, width), BF),
             pltpu.VMEM((1, width), F32),
             pltpu.VMEM((1, width), F32),
             pltpu.VMEM((2, n), jnp.int32),
+            pltpu.VMEM((2, n), F32),
             pltpu.VMEM((n, width), BF),
-            pltpu.SemaphoreType.DMA((3 + PARTS,)),
+            pltpu.VMEM((8, n), F32),
+            pltpu.SMEM((1,), jnp.int32),
+            pltpu.SemaphoreType.DMA((4 + PARTS,)),
         ],
         compiler_params=pltpu.CompilerParams(vmem_limit_bytes=14 * MB),
         name="pack",
-    )(*[stay(a) for a in (tokens, gain.reshape(1, -1), bias.reshape(1, -1), ids.T)])
+    )(*[stay(a) for a in (tokens, gain.reshape(1, -1), bias.reshape(1, -1), ids.T, weight.T)])
 
 
 def expert_kernel(x, ga, gb, ua, ub, da, db, mark, out):
@@ -117,25 +156,21 @@
     )(x, *weights, mark)
 
 
-def mix_kernel(ret, ids_t, weight_t, out, side, done, sems):
+def mix_kernel(ret, ids_t, weight_t, early_pick, out, side, pick, done, sems):
     rows = ret.shape[0]
-    n, width = out.shape
-    place = place_rows(ids_t[...], rows // CAP, CAP)
-    side[...] = jnp.zeros(side.shape, F32)
-    for k in range(2):
-        side[k : k + 1, :] = place[k].astype(F32)
-        side[2 + k : 3 + k, :] = weight_t[k : k + 1, :]
-    cols = side[...].T
-    r = lax.broadcasted_iota(jnp.int32, (n, rows), 1)
-    pick = [
-        jnp.where(r == cols[:, k : k + 1].astype(jnp.int32), 1.0, 0.0).astype(BF) for k in range(2)
-    ]
+    _, width = out.shape
+
+    @pl.when(lax.axis_index("tp") == LAST)
+    def _():
+        pick[...] = early_pick[...]
+
+    @pl.when(lax.axis_index("tp") != LAST)
+    def _():
+        picks(place_rows(ids_t[...], rows // CAP, CAP), weight_t, side, pick)
+
     for i in range(TILES):
         at = pl.ds(i * (width // TILES), width // TILES)
-        part = ret[:, at]
-        done[:, at] = (
-            dot(pick[0], part) * cols[:, 2:3] + dot(pick[1], part) * cols[:, 3:4]
-        ).astype(BF)
+        done[:, at] = dot(pick[...], ret[:, at]).astype(BF)
         pltpu.make_async_copy(done.at[:, at], out.at[:, at], sems.at[i]).start()
     for i in range(TILES):
         at = pl.ds(i * (width // TILES), width // TILES)
@@ -145,21 +180,23 @@
 TILES = 4
 
 
-def mix(ret, ids, weight):
+def mix(ret, ids, weight, pick):
     n = ids.shape[0]
+    rows, width = ret.shape
     return pl.pallas_call(
         mix_kernel,
-        in_specs=[VM] * 3,
+        in_specs=[VM] * 4,
         out_specs=HB,
-        out_shape=jax.ShapeDtypeStruct((n, ret.shape[1]), BF),
+        out_shape=jax.ShapeDtypeStruct((n, width), BF),
         scratch_shapes=[
             pltpu.VMEM((8, n), F32),
-            pltpu.VMEM((n, ret.shape[1]), BF),
+            pltpu.VMEM((n, rows), BF),
+            pltpu.VMEM((n, width), BF),
             pltpu.SemaphoreType.DMA((TILES,)),
         ],
         compiler_params=pltpu.CompilerParams(vmem_limit_bytes=14 * MB),
         name="mix",
-    )(ret, ids.T, weight.T)
+    )(ret, ids.T, weight.T, pick)
 
 
 def body(
@@ -171,7 +208,9 @@
     weights = []
     for w in (gate_weight[0], up_weight[0], down_weight[0]):
         weights += [w, lax.ppermute(w, "tp", swap)]
-    buffer = pack(tokens, norm_gain, norm_bias, expert_ids, experts * CAP)
+    buffer, pick = pack(
+        tokens, norm_gain, norm_bias, expert_ids, route_weights, experts * CAP
+    )
     rows = lax.all_to_all(
         buffer.reshape(experts, CAP, width), "ep", split_axis=0, concat_axis=0, tiled=True
     ).reshape(-1, width)
@@ -180,7 +219,7 @@
     returned = lax.all_to_all(
         result.reshape(experts, CAP, width), "ep", split_axis=0, concat_axis=0, tiled=True
     )
-    return mix(returned.reshape(-1, width), expert_ids, route_weights)
+    return mix(returned.reshape(-1, width), expert_ids, route_weights, pick)
 
 
 def solution(mesh):

time: 158 us -> 140 us (0.89)
  the two profiles are of different devices: /device:TPU:0 before, /device:TPU:1 now
where the time goes in v5:
time: 140 us; the launch traced here: 139 us
  Pallas kernels  47.9 us (34%)
  blocking collectives  42.5 us (30%)
  waiting for transfers between devices  29.9 us (21%)
  starting transfers between devices  13 us (9%)
  local copies, waits for them, and re-layouts  5.15 us (4%)
    all_to_all x1, blocking collectives, body(): lax.all_to_all(result.reshape(experts, CAP, width), 'ep', split_axis=0, c...  42.5 us
    all_to_all x1, waiting for transfers between devices, body(): lax.all_to_all(buffer.reshape(experts, CAP, width), 'ep', split_axis=0, c...  29.9 us
    pallas_call x1, Pallas kernels, pack(): pl.pallas_call(pack_kernel, in_specs=[HB] * 5, out_specs=[VM] * 2, out_sh...  28.3 us
    pallas_call x1, Pallas kernels, expert(): pl.pallas_call(expert_kernel, in_specs=[VM] * 8, out_specs=VM, out_shape=...  17.5 us
    all_to_all x1, starting transfers between devices, body(): lax.all_to_all(buffer.reshape(experts, CAP, width), 'ep', split_axis=0, c...  12.3 us
    unnamed x12, local copies, waits for them, and re-layouts  5.15 us
  transfers between devices with their start and end apart: 4, of which 1 were waited for; matrix products, arithmetic and copies ran while one was open for 0% of the time, Pallas kernels for 0%

profile of v5, /device:TPU:1, one launch (start us, length us, event | category | flops | bytes accessed | tf_op | source)
XLA Modules:
  0.0 139.4 jit_solution(14860410839997894616)
XLA Ops:
  0.0 28.3 %pack.1 = (bf16[1024,2048]{1,0:T(8,128)(2,1)S(1)}, bf16[256,1024]{1,0:T(8,128)(2,1)S(1)}) custom-call(bf16[256,2048]{1,0:T(8,128)(2,1)} %tok.1, f32[1,2048]{1,0:T(1,128)} %bitcast.24, f32[1,2048]{1,0:T(1,128)} %bitcast.25, s32[2,256]{1,0:T(2,128)} %bitcast.20, f32[2,256]{1,0:T(2,128)} %bitcast.22), custom_call_target="tpu_custom_call" | custom-call | tf_op jit(solution)/shard_map/pack/pallas_call | solution.py:110
  28.4 0.0 copy-start
  28.4 2.0 %copy-done = bf16[1024,2048]{1,0:T(8,128)(2,1)} copy-done((bf16[1024,2048]{1,0:T(8,128)(2,1)}, bf16[1024,2048]{1,0:T(8,128)(2,1)S(1)}, u32[]{:S(2)}) %copy-start) | copy-done | bytes 4194328
  30.3 0.0 copy-start.1
  30.3 12.3 %all-to-all-start = ((bf16[64,16,2048]{2,1,0:T(8,128)(2,1)}), bf16[64,16,2048]{2,1,0:T(8,128)(2,1)}, u32[]{:S(2)}, u32[]{:S(2)}) async-start(bf16[64,16,2048]{2,1,0:T(8,128)(2,1)} %bitcast.13), calls=%async_computation | async-start | bytes 8388608 | tf_op jit(solution)/shard_map/all_to_all | solution.py:214
  42.7 0.0 copy-done.1
  42.7 0.1 collective-permute-start
  42.8 0.5 collective-permute-start.1
  43.3 0.1 collective-permute-start.2
  43.4 29.9 %all-to-all-done = bf16[64,16,2048]{2,1,0:T(8,128)(2,1)} async-done(((bf16[64,16,2048]{2,1,0:T(8,128)(2,1)}), bf16[64,16,2048]{2,1,0:T(8,128)(2,1)}, u32[]{:S(2)}, u32[]{:S(2)}) %all-to-all-start) | async-done | bytes 4194336 | tf_op jit(solution)/shard_map/all_to_all | solution.py:214
  73.3 0.7 slice_multiply_fusion.mark
  74.0 0.0 collective-permute-done.gb
  74.0 0.0 collective-permute-done.1.ub
  74.0 0.0 collective-permute-done.2.db
  74.0 0.0 copy-start.2
  74.0 1.6 %copy-done.2 = bf16[1,2048,512]{2,1,0:T(8,128)(2,1)S(1)} copy-done((bf16[1,2048,512]{2,1,0:T(8,128)(2,1)S(1)}, bf16[1,2048,512]{2,1,0:T(8,128)(2,1)}, u32[]{:S(2)}) %copy-start.2) | copy-done | bytes 2097176
  75.6 1.6 %copy-done.3 = bf16[1,512,2048]{2,1,0:T(8,128)(2,1)S(1)} copy-done((bf16[1,512,2048]{2,1,0:T(8,128)(2,1)S(1)}, bf16[1,512,2048]{2,1,0:T(8,128)(2,1)}, u32[]{:S(2)}) %copy-start.3) | copy-done | bytes 2097176
  77.2 17.5 %expert.1 = bf16[1024,2048]{1,0:T(8,128)(2,1)S(1)} custom-call(bf16[1024,2048]{1,0:T(8,128)(2,1)} %bitcast.5.x, bf16[2048,512]{1,0:T(8,128)(2,1)S(1)} %bitcast.15, bf16[2048,512]{1,0:T(8,128)(2,1)} %collective-permute-done.gb, bf16[2048,512]{1,0:T(8,128)(2,1)S(1)} %bitcast.17, bf16[2048,512]{1,0:T(8,128)(2,1)} %collective-permute-done.1.ub, ...), custom_call_target="tpu_custom_call" | custom-call | tf_op jit(solution)/shard_map/expert/pallas_call | solution.py:149
  94.7 0.0 copy-start.4
  94.7 0.0 copy-start.5
  94.7 42.5 %all_to_all.10 = bf16[64,16,2048]{2,1,0:T(8,128)(2,1)S(1)} all-to-all(bf16[64,16,2048]{2,1,0:T(8,128)(2,1)S(1)} %bitcast.12), channel_id=1, replica_groups=mesh['ep'=64,'tp'=2] {'ep'}, dimensions={0} | all-to-all | bytes 8388608 | tf_op jit(solution)/shard_map/all_to_all | solution.py:219
  137.2 0.0 copy-done.4
  137.2 0.0 copy-done.5
  137.2 2.0 %mix.1 = bf16[256,2048]{1,0:T(8,128)(2,1)} custom-call(bf16[1024,2048]{1,0:T(8,128)(2,1)S(1)} %bitcast.11, s32[2,256]{1,0:T(2,128)S(1)} %bitcast.21, f32[2,256]{1,0:T(2,128)S(1)} %bitcast.23, bf16[256,1024]{1,0:T(8,128)(2,1)S(1)} %get-tuple-element.8.early_pick), custom_call_target="tpu_custom_call" | custom-call | tf_op jit(solution)/shard_map/mix/pallas_call | solution.py:186
  (1 shorter events, 0.0 us)
Async XLA Ops:
  28.4 2.0 %copy-start = (bf16[1024,2048]{1,0:T(8,128)(2,1)}, bf16[1024,2048]{1,0:T(8,128)(2,1)S(1)}, u32[]{:S(2)}) copy-start(bf16[1024,2048]{1,0:T(8,128)(2,1)S(1)} %get-tuple-element.7) | copy-start | bytes 12582916
  30.3 12.4 %copy-start.1 = (bf16[1,2048,512]{2,1,0:T(8,128)(2,1)S(1)}, bf16[1,2048,512]{2,1,0:T(8,128)(2,1)}, u32[]{:S(2)}) copy-start(bf16[1,2048,512]{2,1,0:T(8,128)(2,1)} %param.11) | copy-start | bytes 6291460
  30.3 43.0 %all-to-all-start = ((bf16[64,16,2048]{2,1,0:T(8,128)(2,1)}), bf16[64,16,2048]{2,1,0:T(8,128)(2,1)}, u32[]{:S(2)}, u32[]{:S(2)}) async-start(bf16[64,16,2048]{2,1,0:T(8,128)(2,1)} %bitcast.13), calls=%async_computation | async-start | bytes 8388608 | tf_op jit(solution)/shard_map/all_to_all | solution.py:214
  42.7 31.3 %collective-permute-start = (bf16[2048,512]{1,0:T(8,128)(2,1)S(1)}, bf16[2048,512]{1,0:T(8,128)(2,1)}, u32[]{:S(2)}, u32[]{:S(2)}) collective-permute-start(bf16[2048,512]{1,0:T(8,128)(2,1)S(1)} %bitcast.14), channel_id=1, source_target_pairs={{0,1},{1,0},{2,3},{3,2},{4,5},{5,4},{6,7},{7,6},{8,9},{9,8},{10,11... | collective-permute-start | bytes 6291464 | tf_op jit(solution)/shard_map/ppermute | solution.py:210
  42.8 31.2 %collective-permute-start.1 = (bf16[2048,512]{1,0:T(8,128)(2,1)}, bf16[2048,512]{1,0:T(8,128)(2,1)}, u32[]{:S(2)}, u32[]{:S(2)}) collective-permute-start(bf16[2048,512]{1,0:T(8,128)(2,1)} %bitcast.16), channel_id=1, source_target_pairs={{0,1},{1,0},{2,3},{3,2},{4,5},{5,4},{6,7},{7,6},{8,9},{9,8},{10,11... | collective-permute-start | bytes 6291464 | tf_op jit(solution)/shard_map/ppermute | solution.py:210
  43.3 30.7 %collective-permute-start.2 = (bf16[512,2048]{1,0:T(8,128)(2,1)}, bf16[512,2048]{1,0:T(8,128)(2,1)}, u32[]{:S(2)}, u32[]{:S(2)}) collective-permute-start(bf16[512,2048]{1,0:T(8,128)(2,1)} %bitcast.18), channel_id=1, source_target_pairs={{0,1},{1,0},{2,3},{3,2},{4,5},{5,4},{6,7},{7,6},{8,9},{9,8},{10,11... | collective-permute-start | bytes 6291464 | tf_op jit(solution)/shard_map/ppermute | solution.py:210
  74.0 1.6 %copy-start.2 = (bf16[1,2048,512]{2,1,0:T(8,128)(2,1)S(1)}, bf16[1,2048,512]{2,1,0:T(8,128)(2,1)}, u32[]{:S(2)}) copy-start(bf16[1,2048,512]{2,1,0:T(8,128)(2,1)} %param.12) | copy-start | bytes 6291460
  75.6 1.6 %copy-start.3 = (bf16[1,512,2048]{2,1,0:T(8,128)(2,1)S(1)}, bf16[1,512,2048]{2,1,0:T(8,128)(2,1)}, u32[]{:S(2)}) copy-start(bf16[1,512,2048]{2,1,0:T(8,128)(2,1)} %param.13) | copy-start | bytes 6291460
  94.7 42.5 %copy-start.4 = (s32[256,2]{0,1:T(2,128)S(1)}, s32[256,2]{0,1:T(2,128)}, u32[]{:S(2)}) copy-start(s32[256,2]{0,1:T(2,128)} %param.14) | copy-start | bytes 6148
  94.7 42.5 %copy-start.5 = (f32[256,2]{0,1:T(2,128)S(1)}, f32[256,2]{0,1:T(2,128)}, u32[]{:S(2)}) copy-start(f32[256,2]{0,1:T(2,128)} %param.15) | copy-start | bytes 6148

commit v6 on v5

--- a/solution.py
+++ b/solution.py
@@ -96,8 +96,8 @@
         buf[s : s + tile, :] = dot(jnp.where(hit, 1.0, 0.0).astype(BF), normed[...]).astype(BF)
 
 
-PARTS = 4
-HOLD = 2900
+PARTS = 2
+HOLD = 2820
 LAST = 1
 HB = pl.BlockSpec(memory_space=pltpu.HBM)
 VM = pl.BlockSpec(memory_space=pltpu.VMEM)
@@ -177,7 +177,7 @@
         pltpu.make_async_copy(done.at[:, at], out.at[:, at], sems.at[i]).wait()
 
 
-TILES = 4
+TILES = 2
 
 
 def mix(ret, ids, weight, pick):

time: 140 us -> 144 us (1.029)
  blocking collectives: 42.5 us -> 47.7 us
    all_to_all x1, blocking collectives: 42.5 us -> 47.7 us  [body(): lax.all_to_all(result.reshape(experts, CAP, width), 'ep', split_axis=0, c...]
where the time goes in v6:
time: 144 us
  blocking collectives  47.7 us (33%)
  Pallas kernels  47 us (33%)
  waiting for transfers between devices  30 us (21%)
  starting transfers between devices  13 us (9%)
  local copies, waits for them, and re-layouts  5.15 us (4%)
    all_to_all x1, blocking collectives, body(): lax.all_to_all(result.reshape(experts, CAP, width), 'ep', split_axis=0, c...  47.7 us
    all_to_all x1, waiting for transfers between devices, body(): lax.all_to_all(buffer.reshape(experts, CAP, width), 'ep', split_axis=0, c...  30 us
    pallas_call x1, Pallas kernels, pack(): pl.pallas_call(pack_kernel, in_specs=[HB] * 5, out_specs=[VM] * 2, out_sh...  27.3 us
    pallas_call x1, Pallas kernels, expert(): pl.pallas_call(expert_kernel, in_specs=[VM] * 8, out_specs=VM, out_shape=...  17.6 us
    all_to_all x1, starting transfers between devices, body(): lax.all_to_all(buffer.reshape(experts, CAP, width), 'ep', split_axis=0, c...  12.3 us
    unnamed x12, local copies, waits for them, and re-layouts  5.15 us
  transfers between devices with their start and end apart: 4, of which 1 were waited for; matrix products, arithmetic and copies ran while one was open for 0% of the time, Pallas kernels for 0%

profile of v6, /device:TPU:1, one launch (start us, length us, event | category | flops | bytes accessed | tf_op | source)
XLA Modules:
  0.0 143.8 jit_solution(16844341142393890505)
XLA Ops:
  0.0 27.3 %pack.1 = (bf16[1024,2048]{1,0:T(8,128)(2,1)S(1)}, bf16[256,1024]{1,0:T(8,128)(2,1)S(1)}) custom-call(bf16[256,2048]{1,0:T(8,128)(2,1)} %tok.1, f32[1,2048]{1,0:T(1,128)} %bitcast.24, f32[1,2048]{1,0:T(1,128)} %bitcast.25, s32[2,256]{1,0:T(2,128)} %bitcast.20, f32[2,256]{1,0:T(2,128)} %bitcast.22), custom_call_target="tpu_custom_call" | custom-call | tf_op jit(solution)/shard_map/pack/pallas_call | solution.py:110
  27.3 0.0 copy-start
  27.3 2.0 %copy-done = bf16[1024,2048]{1,0:T(8,128)(2,1)} copy-done((bf16[1024,2048]{1,0:T(8,128)(2,1)}, bf16[1024,2048]{1,0:T(8,128)(2,1)S(1)}, u32[]{:S(2)}) %copy-start) | copy-done | bytes 4194328
  29.3 0.0 copy-start.1
  29.3 12.3 %all-to-all-start = ((bf16[64,16,2048]{2,1,0:T(8,128)(2,1)}), bf16[64,16,2048]{2,1,0:T(8,128)(2,1)}, u32[]{:S(2)}, u32[]{:S(2)}) async-start(bf16[64,16,2048]{2,1,0:T(8,128)(2,1)} %bitcast.13), calls=%async_computation | async-start | bytes 8388608 | tf_op jit(solution)/shard_map/all_to_all | solution.py:214
  41.6 0.0 copy-done.1
  41.6 0.1 collective-permute-start
  41.7 0.5 collective-permute-start.1
  42.2 0.1 collective-permute-start.2
  42.3 30.0 %all-to-all-done = bf16[64,16,2048]{2,1,0:T(8,128)(2,1)} async-done(((bf16[64,16,2048]{2,1,0:T(8,128)(2,1)}), bf16[64,16,2048]{2,1,0:T(8,128)(2,1)}, u32[]{:S(2)}, u32[]{:S(2)}) %all-to-all-start) | async-done | bytes 4194336 | tf_op jit(solution)/shard_map/all_to_all | solution.py:214
  72.3 0.7 slice_multiply_fusion.mark
  73.0 0.0 collective-permute-done.gb
  73.0 0.0 collective-permute-done.1.ub
  73.0 0.0 collective-permute-done.2.db
  73.0 0.0 copy-start.2
  73.0 1.6 %copy-done.2 = bf16[1,2048,512]{2,1,0:T(8,128)(2,1)S(1)} copy-done((bf16[1,2048,512]{2,1,0:T(8,128)(2,1)S(1)}, bf16[1,2048,512]{2,1,0:T(8,128)(2,1)}, u32[]{:S(2)}) %copy-start.2) | copy-done | bytes 2097176
  74.6 1.6 %copy-done.3 = bf16[1,512,2048]{2,1,0:T(8,128)(2,1)S(1)} copy-done((bf16[1,512,2048]{2,1,0:T(8,128)(2,1)S(1)}, bf16[1,512,2048]{2,1,0:T(8,128)(2,1)}, u32[]{:S(2)}) %copy-start.3) | copy-done | bytes 2097176
  76.2 17.6 %expert.1 = bf16[1024,2048]{1,0:T(8,128)(2,1)S(1)} custom-call(bf16[1024,2048]{1,0:T(8,128)(2,1)} %bitcast.5.x, bf16[2048,512]{1,0:T(8,128)(2,1)S(1)} %bitcast.15, bf16[2048,512]{1,0:T(8,128)(2,1)} %collective-permute-done.gb, bf16[2048,512]{1,0:T(8,128)(2,1)S(1)} %bitcast.17, bf16[2048,512]{1,0:T(8,128)(2,1)} %collective-permute-done.1.ub, ...), custom_call_target="tpu_custom_call" | custom-call | tf_op jit(solution)/shard_map/expert/pallas_call | solution.py:149
  93.8 0.0 copy-start.4
  93.8 0.0 copy-start.5
  93.8 47.7 %all_to_all.10 = bf16[64,16,2048]{2,1,0:T(8,128)(2,1)S(1)} all-to-all(bf16[64,16,2048]{2,1,0:T(8,128)(2,1)S(1)} %bitcast.12), channel_id=1, replica_groups=mesh['ep'=64,'tp'=2] {'ep'}, dimensions={0} | all-to-all | bytes 8388608 | tf_op jit(solution)/shard_map/all_to_all | solution.py:219
  141.5 0.0 copy-done.4
  141.5 0.0 copy-done.5
  141.5 2.1 %mix.1 = bf16[256,2048]{1,0:T(8,128)(2,1)} custom-call(bf16[1024,2048]{1,0:T(8,128)(2,1)S(1)} %bitcast.11, s32[2,256]{1,0:T(2,128)S(1)} %bitcast.21, f32[2,256]{1,0:T(2,128)S(1)} %bitcast.23, bf16[256,1024]{1,0:T(8,128)(2,1)S(1)} %get-tuple-element.8.early_pick), custom_call_target="tpu_custom_call" | custom-call | tf_op jit(solution)/shard_map/mix/pallas_call | solution.py:186
  (1 shorter events, 0.0 us)
Async XLA Ops:
  27.3 2.0 %copy-start = (bf16[1024,2048]{1,0:T(8,128)(2,1)}, bf16[1024,2048]{1,0:T(8,128)(2,1)S(1)}, u32[]{:S(2)}) copy-start(bf16[1024,2048]{1,0:T(8,128)(2,1)S(1)} %get-tuple-element.7) | copy-start | bytes 12582916
  29.3 12.4 %copy-start.1 = (bf16[1,2048,512]{2,1,0:T(8,128)(2,1)S(1)}, bf16[1,2048,512]{2,1,0:T(8,128)(2,1)}, u32[]{:S(2)}) copy-start(bf16[1,2048,512]{2,1,0:T(8,128)(2,1)} %param.11) | copy-start | bytes 6291460
  29.3 43.0 %all-to-all-start = ((bf16[64,16,2048]{2,1,0:T(8,128)(2,1)}), bf16[64,16,2048]{2,1,0:T(8,128)(2,1)}, u32[]{:S(2)}, u32[]{:S(2)}) async-start(bf16[64,16,2048]{2,1,0:T(8,128)(2,1)} %bitcast.13), calls=%async_computation | async-start | bytes 8388608 | tf_op jit(solution)/shard_map/all_to_all | solution.py:214
  41.6 31.4 %collective-permute-start = (bf16[2048,512]{1,0:T(8,128)(2,1)S(1)}, bf16[2048,512]{1,0:T(8,128)(2,1)}, u32[]{:S(2)}, u32[]{:S(2)}) collective-permute-start(bf16[2048,512]{1,0:T(8,128)(2,1)S(1)} %bitcast.14), channel_id=1, source_target_pairs={{0,1},{1,0},{2,3},{3,2},{4,5},{5,4},{6,7},{7,6},{8,9},{9,8},{10,11... | collective-permute-start | bytes 6291464 | tf_op jit(solution)/shard_map/ppermute | solution.py:210
  41.7 31.3 %collective-permute-start.1 = (bf16[2048,512]{1,0:T(8,128)(2,1)}, bf16[2048,512]{1,0:T(8,128)(2,1)}, u32[]{:S(2)}, u32[]{:S(2)}) collective-permute-start(bf16[2048,512]{1,0:T(8,128)(2,1)} %bitcast.16), channel_id=1, source_target_pairs={{0,1},{1,0},{2,3},{3,2},{4,5},{5,4},{6,7},{7,6},{8,9},{9,8},{10,11... | collective-permute-start | bytes 6291464 | tf_op jit(solution)/shard_map/ppermute | solution.py:210
  42.2 30.8 %collective-permute-start.2 = (bf16[512,2048]{1,0:T(8,128)(2,1)}, bf16[512,2048]{1,0:T(8,128)(2,1)}, u32[]{:S(2)}, u32[]{:S(2)}) collective-permute-start(bf16[512,2048]{1,0:T(8,128)(2,1)} %bitcast.18), channel_id=1, source_target_pairs={{0,1},{1,0},{2,3},{3,2},{4,5},{5,4},{6,7},{7,6},{8,9},{9,8},{10,11... | collective-permute-start | bytes 6291464 | tf_op jit(solution)/shard_map/ppermute | solution.py:210
  73.0 1.6 %copy-start.2 = (bf16[1,2048,512]{2,1,0:T(8,128)(2,1)S(1)}, bf16[1,2048,512]{2,1,0:T(8,128)(2,1)}, u32[]{:S(2)}) copy-start(bf16[1,2048,512]{2,1,0:T(8,128)(2,1)} %param.12) | copy-start | bytes 6291460
  74.6 1.6 %copy-start.3 = (bf16[1,512,2048]{2,1,0:T(8,128)(2,1)S(1)}, bf16[1,512,2048]{2,1,0:T(8,128)(2,1)}, u32[]{:S(2)}) copy-start(bf16[1,512,2048]{2,1,0:T(8,128)(2,1)} %param.13) | copy-start | bytes 6291460
  93.8 47.7 %copy-start.4 = (s32[256,2]{0,1:T(2,128)S(1)}, s32[256,2]{0,1:T(2,128)}, u32[]{:S(2)}) copy-start(s32[256,2]{0,1:T(2,128)} %param.14) | copy-start | bytes 6148
  93.8 47.7 %copy-start.5 = (f32[256,2]{0,1:T(2,128)S(1)}, f32[256,2]{0,1:T(2,128)}, u32[]{:S(2)}) copy-start(f32[256,2]{0,1:T(2,128)} %param.15) | copy-start | bytes 6148
